TPU v7x, 256 devices: a whole 4x4x8 slice. The times are simulated.
256 devices in a mesh: ep: 16 (over y, x), tp: 16 (over z, core).
Axes of the slice: x: 4, y: 4, z: 8, core: 2. Of those that a mesh axis runs over, the one named last changes fastest.
Arguments:
- tokens: bfloat16 [512, 4096], P('ep'), may hold values from -6 to 6
- state_matrix: float32 [512, 16, 128, 128], P('ep', 'tp'), may hold values from -1.5 to 1.5
- state_norm: float32 [512, 16, 128], P('ep', 'tp'), may hold values from -4 to 4
- state_max: float32 [512, 16], P('ep', 'tp'), may hold values from -5 to 5
- mixer_gain: float32 [4096], replicated, may hold values from 0.1 to 1.9
- w_query: bfloat16 [4096, 2048], P('ep', 'tp'), may hold values from -0.09375 to 0.09375
- w_key: bfloat16 [4096, 2048], P('ep', 'tp'), may hold values from -0.09375 to 0.09375
- w_value: bfloat16 [4096, 2048], P('ep', 'tp'), may hold values from -0.09375 to 0.09375
- w_outgate: bfloat16 [4096, 2048], P('ep', 'tp'), may hold values from -0.09375 to 0.09375
- w_ingate: bfloat16 [4096, 16], replicated, may hold values from -0.09375 to 0.09375
- w_forget: bfloat16 [4096, 16], replicated, may hold values from -0.09375 to 0.09375
- forget_bias: float32 [16], replicated, may hold values from -2 to 4
- w_proj: bfloat16 [2048, 4096], P('tp', 'ep'), may hold values from -0.125 to 0.125
- ffn_gain: float32 [4096], replicated, may hold values from 0.1 to 1.9
- w_branch: bfloat16 [4096], replicated, may hold values from -0.09375 to 0.09375
- routes: int32 [512, 2], P('ep'), may hold values from 0 to 15, all different within a row; in each aligned block of 32 rows (0 to 31, 32 to 63, ...) at most 6 rows name the same one
- route_weight: float32 [512, 2], P('ep'), may hold values from 0.2 to 1
- expert_gate: bfloat16 [16, 4096, 4096], P('ep', None, 'tp'), may hold values from -0.09375 to 0.09375
- expert_up: bfloat16 [16, 4096, 4096], P('ep', None, 'tp'), may hold values from -0.09375 to 0.09375
- expert_down: bfloat16 [16, 4096, 4096], P('ep', 'tp'), may hold values from -0.09375 to 0.09375
- dense_gate: bfloat16 [4096, 8192], P('ep', 'tp'), may hold values from -0.09375 to 0.09375
- dense_up: bfloat16 [4096, 8192], P('ep', 'tp'), may hold values from -0.09375 to 0.09375
- dense_down: bfloat16 [8192, 4096], P('tp', 'ep'), may hold values from -0.0625 to 0.0625
Outputs:
- layer_out: bfloat16 [512, 4096], P('ep')
- new_matrix: float32 [512, 16, 128, 128], P('ep', 'tp')
- new_norm: float32 [512, 16, 128], P('ep', 'tp')
- new_max: float32 [512, 16], P('ep', 'tp')
Inputs may be any that keep to these rules, and one draw needn't show every extreme that they name: `routes`: each row names 2 different experts. Among the rows of one index of ep (32 sequences) no expert is named more than 6 times, and in some such group one expert is named exactly 6 times.
All inputs are finite; a program needn't handle non-finite values.
Results may differ from a plain program's by a relative error of at most 0.012.
Values may be sent and summed in bfloat16 or wider, within the bound.
A program may use at most 64 MiB of HBM per device.

v0:
```python
import functools

import jax
import jax.numpy as jnp
from jax import lax
from jax.experimental import pallas as pl
from jax.experimental.pallas import tpu as pltpu
from jax.sharding import PartitionSpec as P

EPS = 1e-06
LANES = 128
F32 = jnp.float32
BF16 = jnp.bfloat16


def layer_kernel(
    n_ep,
    n_tp,
    tokens_ref,
    aux_gain_ref,
    gate_w_ref,
    gate_b_ref,
    state_norm_ref,
    state_max_ref,
    ffn_gain_ref,
    branch_ref,
    routes_ref,
    weight_ref,
    state_hbm,
    wq_hbm,
    wk_hbm,
    wv_hbm,
    wo_hbm,
    wproj_hbm,
    eg_hbm,
    eu_hbm,
    ed_hbm,
    dg_hbm,
    du_hbm,
    dd_hbm,
    out_ref,
    norm_out_ref,
    max_out_ref,
    keyw_ref,
    value_ref,
    keep_ref,
    state,
    wcat,
    wproj,
    eg,
    eu,
    ed,
    dg,
    du,
    dd,
    raw_all,
    aux,
    aux_all,
    xblock,
    part_send,
    part_recv,
    numer,
    mixed_all,
    proj_send,
    proj_recv,
    res_block,
    res_full,
    dense_send,
    dense_recv,
    hid_all,
    ehid,
    acc,
    fin_send,
    fin_recv,
    tp_send,
    tp_recv,
    out_all,
    load_sems,
    send_ep,
    recv_ep,
    send_tp,
    recv_tp,
):
    e = lax.axis_index("ep")
    t = lax.axis_index("tp")
    R, D = tokens_ref.shape
    N = R * n_ep
    Dc = D // n_ep
    Dt = D // n_tp
    Nt = N // n_tp
    H, hd = state_norm_ref.shape[1], state_norm_ref.shape[2]
    W = H * hd
    F = dg.shape[1]
    LE, FE = eg.shape[0], eg.shape[2]

    loads = []

    def load(src, dst):
        copy = pltpu.make_async_copy(src, dst, load_sems.at[len(loads)])
        copy.start()
        loads.append(copy)
        return copy

    def at(index, size):
        return pl.ds(pl.multiple_of(index * size, size), size)

    def ep_copy(phase, k, src, dst):
        peer = lax.rem(e + k, n_ep)
        return pltpu.make_async_remote_copy(
            src_ref=src(peer),
            dst_ref=dst,
            send_sem=send_ep.at[phase, k],
            recv_sem=recv_ep.at[phase, k],
            device_id={"ep": peer},
            device_id_type=pl.DeviceIdType.MESH,
        )

    def tp_copy(phase, k, src, dst):
        peer = lax.rem(t + k, n_tp)
        return pltpu.make_async_remote_copy(
            src_ref=src(peer),
            dst_ref=dst,
            send_sem=send_tp.at[phase, k],
            recv_sem=recv_tp.at[phase, k],
            device_id={"tp": peer},
            device_id_type=pl.DeviceIdType.MESH,
        )

    pending = []

    def start_all(kind, phase, src, dst):
        count = n_ep if kind is ep_copy else n_tp
        copies = [kind(phase, k, src, dst) for k in range(1, count)]
        for copy in copies:
            copy.start()
        pending.extend(copies)
        return copies

    def arrive(copies):
        for copy in copies:
            copy.wait_recv()

    barrier = pltpu.get_barrier_semaphore()
    for k in range(1, n_ep):
        pl.semaphore_signal(
            barrier,
            inc=1,
            device_id={"ep": lax.rem(e + k, n_ep)},
            device_id_type=pl.DeviceIdType.MESH,
        )
    for k in range(1, n_tp):
        pl.semaphore_signal(
            barrier,
            inc=1,
            device_id={"tp": lax.rem(t + k, n_tp)},
            device_id_type=pl.DeviceIdType.MESH,
        )

    load_w = [
        load(src, wcat.at[:, pl.ds(i * W, W)])
        for i, src in enumerate((wq_hbm, wk_hbm, wv_hbm, wo_hbm))
    ]
    load_state = load(state_hbm, state)
    load_proj = load(wproj_hbm, wproj)
    load_dg, load_du = load(dg_hbm, dg), load(du_hbm, du)
    load_eg, load_eu = load(eg_hbm, eg), load(eu_hbm, eu)
    load_ed, load_dd = load(ed_hbm, ed), load(dd_hbm, dd)

    wide = tokens_ref[...].astype(F32)
    scale = lax.rsqrt(jnp.mean(wide * wide, axis=-1, keepdims=True) + EPS)
    lane = lax.broadcasted_iota(jnp.int32, (R, LANES), 1)
    weights = weight_ref[...]
    shares = weights / jnp.sum(weights, axis=1, keepdims=True)
    share_map = jnp.zeros((R, LANES), F32)
    for k in range(weights.shape[1]):
        share_map += jnp.where(lane == routes_ref[:, k : k + 1], shares[:, k : k + 1], 0.0)
    aux[:, 0:LANES] = share_map
    aux[:, LANES : 2 * LANES] = jnp.broadcast_to(scale, (R, LANES))

    pl.semaphore_wait(barrier, n_ep - 1 + n_tp - 1)
    sent_raw = start_all(
        ep_copy, 0, lambda p: tokens_ref.at[:, at(p, Dc)], raw_all.at[at(e, R), :]
    )
    sent_aux = start_all(ep_copy, 1, lambda p: aux, aux_all.at[at(e, R), :])
    raw_all[at(e, R), :] = tokens_ref[:, at(e, Dc)]
    aux_all[at(e, R), :] = aux[...]

    normed = (wide * scale * aux_gain_ref[...]).astype(BF16)
    gates = (
        lax.dot_general(
            normed, gate_w_ref[...], (((1,), (1,)), ((), ())), preferred_element_type=F32
        )
        + gate_b_ref[...]
    )
    gate_lane = lax.broadcasted_iota(jnp.int32, gates.shape, 1)
    heads_all = gates.shape[1] // 2

    arrive(sent_raw)
    arrive(sent_aux)
    xblock[...] = (
        raw_all[...].astype(F32) * aux_all[:, LANES : LANES + 1] * aux_gain_ref[:, at(e, Dc)]
    ).astype(BF16)
    for copy in load_w:
        copy.wait()
    part_send[...] = jnp.dot(xblock[...], wcat[...], preferred_element_type=F32).astype(BF16)
    sent_part = start_all(ep_copy, 2, lambda p: part_send.at[at(p, R), :], part_recv.at[e])
    part_recv[e] = part_send[at(e, R), :]
    arrive(sent_part)
    proj = part_recv[0].astype(F32)
    for i in range(1, n_ep):
        proj += part_recv[i].astype(F32)

    load_state.wait()
    for h in range(H):
        lo, hi = h * hd, (h + 1) * hd
        q = proj[:, lo:hi]
        key = proj[:, W + lo : W + hi] * hd ** (-0.5)
        val = proj[:, 2 * W + lo : 2 * W + hi]
        og = proj[:, 3 * W + lo : 3 * W + hi]
        g_in = jnp.sum(jnp.where(gate_lane == t * H + h, gates, 0.0), axis=1, keepdims=True)
        g_fo = jnp.sum(
            jnp.where(gate_lane == heads_all + t * H + h, gates, 0.0), axis=1, keepdims=True
        )
        log_keep = jnp.minimum(g_fo, 0.0) - jnp.log(1.0 + jnp.exp(-jnp.abs(g_fo)))
        carried = log_keep + state_max_ref[:, h : h + 1]
        new_max = jnp.maximum(carried, g_in)
        keep = jnp.exp(carried - new_max)
        write = jnp.exp(g_in - new_max)
        key_w = write * key
        new_norm = keep * state_norm_ref[:, h, :] + key_w
        q_t = q.T
        for b in range(R):
            numer[b : b + 1, :] = jnp.sum(q_t[:, b : b + 1] * state[b, h], axis=0, keepdims=True)
        top = keep * numer[...] + jnp.sum(q * key_w, axis=1, keepdims=True) * val
        denom = jnp.sum(q * new_norm, axis=1, keepdims=True)
        cell = top / jnp.maximum(jnp.abs(denom), 1.0)
        mixed_all[at(e, R), lo:hi] = (cell / (1.0 + jnp.exp(-og))).astype(BF16)
        norm_out_ref[:, h, :] = new_norm
        max_out_ref[:, h : h + 1] = new_max
        keyw_ref[:, h, :] = key_w
        value_ref[:, h, :] = val
        keep_ref[:, h : h + 1] = keep

    sent_mixed = start_all(
        ep_copy, 3, lambda p: mixed_all.at[at(e, R), :], mixed_all.at[at(e, R), :]
    )
    load_proj.wait()
    arrive(sent_mixed)
    proj_send[...] = jnp.dot(mixed_all[...], wproj[...], preferred_element_type=F32).astype(BF16)
    sent_proj = start_all(tp_copy, 0, lambda p: proj_send.at[at(p, Nt), :], proj_recv.at[t])
    proj_recv[t] = proj_send[at(t, Nt), :]
    arrive(sent_proj)
    total = raw_all[at(t, Nt), :].astype(F32)
    for i in range(n_tp):
        total += proj_recv[i].astype(F32)
    res_block[at(t, Nt), :] = total.astype(BF16)
    sent_res = start_all(tp_copy, 1, lambda p: res_block.at[at(t, Nt), :], res_block.at[at(t, Nt), :])
    arrive(sent_res)
    sent_full = start_all(ep_copy, 4, lambda p: res_block, res_full.at[:, at(e, Dc)])
    res_full[:, at(e, Dc)] = res_block[...]

    xblock[...] = (res_block[...].astype(F32) * ffn_gain_ref[:, at(e, Dc)]).astype(BF16)
    load_dg.wait()
    load_du.wait()
    chunk = min(512, F)

    def dense_in(c, _):
        cols = at(c, chunk)
        dense_send[:, cols] = jnp.dot(
            xblock[...], dg[:, cols], preferred_element_type=F32
        ).astype(BF16)
        dense_send[:, pl.ds(pl.multiple_of(F + c * chunk, chunk), chunk)] = jnp.dot(
            xblock[...], du[:, cols], preferred_element_type=F32
        ).astype(BF16)
        return _

    lax.fori_loop(0, F // chunk, dense_in, 0)
    sent_dense = start_all(ep_copy, 5, lambda p: dense_send.at[at(p, R), :], dense_recv.at[e])
    dense_recv[e] = dense_send[at(e, R), :]

    arrive(sent_full)
    mine = res_full[at(e, R), :].astype(F32)
    my_scale = lax.rsqrt(jnp.mean(mine * mine, axis=-1, keepdims=True) + EPS)
    arrive(sent_dense)
    both = dense_recv[0].astype(F32)
    for i in range(1, n_ep):
        both += dense_recv[i].astype(F32)
    both *= my_scale
    g, u = both[:, :F], both[:, F:]
    hid_all[at(e, R), :] = (g / (1.0 + jnp.exp(-g)) * u).astype(BF16)
    sent_hid = start_all(ep_copy, 6, lambda p: hid_all.at[at(e, R), :], hid_all.at[at(e, R), :])

    def norm_rows(c, _):
        rows = at(c, R)
        block = res_full[rows, :].astype(F32)
        row_scale = lax.rsqrt(jnp.mean(block * block, axis=-1, keepdims=True) + EPS)
        ffn = (block * row_scale * ffn_gain_ref[...]).astype(BF16)
        fin_send[rows, :] = ffn
        gate = jnp.sum(ffn.astype(F32) * branch_ref[...].astype(F32), axis=1, keepdims=True)
        aux_all[rows, LANES : 2 * LANES] = jnp.broadcast_to(
            1.0 / (1.0 + jnp.exp(-gate)), (R, LANES)
        )
        return _

    lax.fori_loop(0, n_ep, norm_rows, 0)

    load_eg.wait()
    load_eu.wait()
    all_lane = lax.broadcasted_iota(jnp.int32, (N, LANES), 1)
    half = min(256, FE)
    for le in range(LE):

        def expert_in(c, _):
            cols = at(c, half)
            gp = jnp.dot(fin_send[...], eg[le, :, cols], preferred_element_type=F32)
            up = jnp.dot(fin_send[...], eu[le, :, cols], preferred_element_type=F32)
            ehid[le, :, cols] = (gp / (1.0 + jnp.exp(-gp)) * up).astype(BF16)
            return _

        lax.fori_loop(0, FE // half, expert_in, 0)
    load_ed.wait()
    wide_cols = min(512, D)
    for le in range(LE):
        share = jnp.sum(
            jnp.where(all_lane == e * LE + le, aux_all[:, 0:LANES], 0.0), axis=1, keepdims=True
        )

        def expert_out(c, _):
            cols = at(c, wide_cols)
            term = share * jnp.dot(ehid[le], ed[le, :, cols], preferred_element_type=F32)
            if le == 0:
                acc[:, cols] = term
            else:
                acc[:, cols] += term
            return _

        lax.fori_loop(0, D // wide_cols, expert_out, 0)

    load_dd.wait()
    arrive(sent_hid)
    own = at(e, Dc)
    acc[:, own] += aux_all[:, LANES : LANES + 1] * jnp.dot(
        hid_all[...], dd[...], preferred_element_type=F32
    )

    def narrow(c, _):
        rows = at(c, R)
        fin_send[rows, :] = acc[rows, :].astype(BF16)
        return _

    lax.fori_loop(0, n_ep, narrow, 0)
    sent_fin = start_all(ep_copy, 7, lambda p: fin_send.at[at(p, R), :], fin_recv.at[e])
    fin_recv[e] = fin_send[at(e, R), :]
    arrive(sent_fin)
    part = fin_recv[0].astype(F32)
    for i in range(1, n_ep):
        part += fin_recv[i].astype(F32)
    tp_send[...] = part.astype(BF16)
    sent_tp = start_all(tp_copy, 2, lambda p: tp_send.at[:, at(p, Dt)], tp_recv.at[t])
    tp_recv[t] = tp_send[:, at(t, Dt)]
    arrive(sent_tp)
    last = res_full[at(e, R), at(t, Dt)].astype(F32)
    for i in range(n_tp):
        last += tp_recv[i].astype(F32)
    out_all[:, at(t, Dt)] = last.astype(BF16)
    sent_out = start_all(
        tp_copy, 3, lambda p: out_all.at[:, at(t, Dt)], out_all.at[:, at(t, Dt)]
    )
    arrive(sent_out)
    out_ref[...] = out_all[...]
    for copy in pending:
        copy.wait_send()


def on_device(
    n_ep,
    n_tp,
    tokens,
    state_matrix,
    state_norm,
    state_max,
    mixer_gain,
    w_query,
    w_key,
    w_value,
    w_outgate,
    w_ingate,
    w_forget,
    forget_bias,
    w_proj,
    ffn_gain,
    w_branch,
    routes,
    route_weight,
    expert_gate,
    expert_up,
    expert_down,
    dense_gate,
    dense_up,
    dense_down,
):
    R, D = tokens.shape
    H, hd = state_norm.shape[1:]
    N, Dc, Dt, W = R * n_ep, D // n_ep, D // n_tp, H * hd
    Nt = N // n_tp
    F = dense_gate.shape[1]
    LE, _, FE = expert_gate.shape
    gate_w = jnp.concatenate([w_ingate.T, w_forget.T], axis=0)
    gate_b = jnp.concatenate([jnp.zeros_like(forget_bias), forget_bias])[None, :]
    vmem = pl.BlockSpec(memory_space=pltpu.VMEM)
    hbm = pl.BlockSpec(memory_space=pl.ANY)
    V = pltpu.VMEM
    scratch = [
        V(state_matrix.shape, F32),
        V((Dc, 4 * W), BF16),
        V(w_proj.shape, BF16),
        V(expert_gate.shape, BF16),
        V(expert_up.shape, BF16),
        V(expert_down.shape, BF16),
        V(dense_gate.shape, BF16),
        V(dense_up.shape, BF16),
        V(dense_down.shape, BF16),
        V((N, Dc), BF16),
        V((R, 2 * LANES), F32),
        V((N, 2 * LANES), F32),
        V((N, Dc), BF16),
        V((N, 4 * W), BF16),
        V((n_ep, R, 4 * W), BF16),
        V((R, hd), F32),
        V((N, W), BF16),
        V((N, Dc), BF16),
        V((n_tp, Nt, Dc), BF16),
        V((N, Dc), BF16),
        V((N, D), BF16),
        V((N, 2 * F), BF16),
        V((n_ep, R, 2 * F), BF16),
        V((N, F), BF16),
        V((LE, N, FE), BF16),
        V((N, D), F32),
        V((N, D), BF16),
        V((n_ep, R, D), BF16),
        V((R, D), BF16),
        V((n_tp, R, Dt), BF16),
        V((R, D), BF16),
        pltpu.SemaphoreType.DMA((12,)),
        pltpu.SemaphoreType.DMA((8, n_ep)),
        pltpu.SemaphoreType.DMA((8, n_ep)),
        pltpu.SemaphoreType.DMA((4, n_tp)),
        pltpu.SemaphoreType.DMA((4, n_tp)),
    ]
    S = jax.ShapeDtypeStruct
    layer_out, new_norm, new_max, key_w, value, keep = pl.pallas_call(
        functools.partial(layer_kernel, n_ep, n_tp),
        out_shape=(
            S((R, D), BF16),
            S((R, H, hd), F32),
            S((R, H), F32),
            S((R, H, hd), F32),
            S((R, H, hd), F32),
            S((R, H), F32),
        ),
        in_specs=[vmem] * 10 + [hbm] * 12,
        out_specs=(vmem,) * 6,
        scratch_shapes=scratch,
        compiler_params=pltpu.CompilerParams(
            collective_id=0, has_side_effects=True, vmem_limit_bytes=66_000_000
        ),
    )(
        tokens,
        mixer_gain[None, :],
        gate_w,
        gate_b,
        state_norm,
        state_max,
        ffn_gain[None, :],
        w_branch[None, :],
        routes,
        route_weight,
        state_matrix,
        w_query,
        w_key,
        w_value,
        w_outgate,
        w_proj,
        expert_gate,
        expert_up,
        expert_down,
        dense_gate,
        dense_up,
        dense_down,
    )
    new_matrix = keep[:, :, None, None] * state_matrix + key_w[:, :, :, None] * value[:, :, None, :]
    return (layer_out, new_matrix, new_norm, new_max)


def solution(mesh):
    in_specs = (
        P("ep", None),
        P("ep", "tp", None, None),
        P("ep", "tp", None),
        P("ep", "tp"),
        P(),
        P("ep", "tp"),
        P("ep", "tp"),
        P("ep", "tp"),
        P("ep", "tp"),
        P(),
        P(),
        P(),
        P("tp", "ep"),
        P(),
        P(),
        P("ep", None),
        P("ep", None),
        P("ep", None, "tp"),
        P("ep", None, "tp"),
        P("ep", "tp", None),
        P("ep", "tp"),
        P("ep", "tp"),
        P("tp", "ep"),
    )
    out_specs = (P("ep", None), P("ep", "tp", None, None), P("ep", "tp", None), P("ep", "tp"))
    return jax.shard_map(
        functools.partial(on_device, mesh.shape["ep"], mesh.shape["tp"]),
        mesh=mesh,
        in_specs=in_specs,
        out_specs=out_specs,
        check_vma=False,
    )
```

profile of v0, /device:TPU:1, one launch (start us, length us, event | category | flops | bytes accessed | tf_op | source)
XLA Modules:
  0.0 256.6 jit_solution(4722756275492160152)
XLA Ops:
  0.6 1.2 pad_bitcast_fusion.gate_b_ref
  1.9 1.3 copy.31.state_max_ref
  3.2 1.3 broadcast_in_dim.18.branch_ref
  4.5 1.4 copy.32.routes_ref
  5.9 1.4 copy.33.weight_ref
  7.2 1.7 pad_maximum_fusion.gate_w_ref
  8.9 241.2 %shard_map.246 = (bf16[32,4096]{1,0:T(8,128)(2,1)}, f32[32,1,128]{2,1,0:T(1,128)}, f32[32,1]{1,0:T(8,128)}, f32[32,1,128]{2,1,0:T(1,128)}, f32[32,1,128]{2,1,0:T(1,128)}, /*index=5*/f32[32,1]{1,0:T(8,128)}) custom-call(bf16[32,4096]{1,0:T(8,128)(2,1)} %tokens_ref.1, f32[1,4096]{1,0:T(1,128)} %bitcast.10, bf16[32,4096]{1,0:T(8,128)(2,1)} %pad_maximum_fusion.gate_w_ref, ...), custom_call_target="tpu_custom_call" | custom-call | tf_op jit(solution)/shard_map/pallas_call | solution.py:452
  250.1 0.8 reduce
  251.0 1.3 copy.34
  252.3 0.0 copy-start
  252.3 0.0 copy-start.1
  252.3 3.0 %multiply_add_fusion = f32[32,1,128,128]{3,2,1,0:T(8,128)} fusion(f32[32,1,128,128]{3,2,1,0:T(8,128)} %state_hbm.1, f32[32,128]{1,0:T(8,128)} %bitcast.13, f32[32,128]{1,0:T(8,128)} %bitcast.12, f32[32]{0:T(128)S(1)} %reduce), kind=kLoop, calls=%fused_computation | loop fusion | flops 1572864 | bytes 4227200 | tf_op jit(solution)/shard_map/add | solution.py:492
  255.3 0.0 copy-done
  255.3 0.7 copy.37
  256.0 0.0 copy-done.1
  256.0 0.6 copy.38
Async XLA Ops:
  252.3 3.0 %copy-start = (bf16[32,4096]{1,0:T(8,128)(2,1)S(1)}, bf16[32,4096]{1,0:T(8,128)(2,1)}, u32[]{:S(2)}) copy-start(bf16[32,4096]{1,0:T(8,128)(2,1)} %get-tuple-element.28) | copy-start | bytes 786436
  252.3 3.7 %copy-start.1 = (f32[32,1,128]{2,1,0:T(1,128)S(1)}, f32[32,1,128]{2,1,0:T(1,128)}, u32[]{:S(2)}) copy-start(f32[32,1,128]{2,1,0:T(1,128)} %get-tuple-element.30) | copy-start | bytes 49156
where the time goes:
time: 257 us
  Pallas kernels  241 us (94%)
  local copies, waits for them, and re-layouts  9.22 us (4%)
  other arithmetic  5.52 us (2%)
    pallas_call x1, Pallas kernels, on_device(): pl.pallas_call(functools.partial(layer_kernel, n_ep, n_tp), out_shape=(S(...  241 us
    unnamed x10, local copies, waits for them, and re-layouts  6.67 us

commit v1 on v0

v1 whole, which is shorter than its diff:
```python
import functools

import jax
import jax.numpy as jnp
from jax import lax
from jax.experimental import pallas as pl
from jax.experimental.pallas import tpu as pltpu
from jax.sharding import PartitionSpec as P

EPS = 1e-06
LANES = 128
CAP = 6
PAD = 8
F32 = jnp.float32
BF16 = jnp.bfloat16
MESH = pl.DeviceIdType.MESH


def dot(a, b):
    return jnp.dot(a, b, preferred_element_type=F32)


def dot_t(a, b):
    return lax.dot_general(a, b, (((1,), (1,)), ((), ())), preferred_element_type=F32)


def iota(shape, dim):
    return lax.broadcasted_iota(jnp.int32, shape, dim)


def layer_kernel(
    n_ep,
    n_tp,
    tokens_ref,
    gain_ref,
    win_ref,
    wfo_ref,
    bias_ref,
    norm_ref,
    smax_ref,
    fgain_ref,
    branch_ref,
    routes_ref,
    weight_ref,
    state_hbm,
    wq_hbm,
    wk_hbm,
    wv_hbm,
    wo_hbm,
    wproj_hbm,
    eg_hbm,
    eu_hbm,
    ed_hbm,
    dg_hbm,
    du_hbm,
    dd_hbm,
    out_ref,
    norm_out_ref,
    max_out_ref,
    keyw_ref,
    value_ref,
    keep_ref,
    state,
    wcat,
    wproj,
    eg,
    eu,
    ed,
    dgu,
    dd,
    nrm,
    x_all,
    info,
    info_recv,
    part_send,
    part_recv,
    numer,
    mix_send,
    mix_all,
    raw_blk,
    res_all,
    res_t,
    xg,
    gmat,
    stat,
    stat_recv,
    dense_send,
    dense_recv,
    disp_send,
    xrecv,
    hid_all,
    fin_send,
    fin_recv,
    dn_send,
    dn_recv,
    tp_send,
    tp_recv,
    out_all,
    load_sems,
    send_ep,
    recv_ep,
    send_tp,
    recv_tp,
    send_mx,
    recv_mx,
    send_tr,
    recv_tr,
):
    e = lax.axis_index("ep")
    t = lax.axis_index("tp")
    R, D = tokens_ref.shape
    N = R * n_ep
    Dc = D // n_ep
    Dt = D // n_tp
    W = mix_send.shape[1]
    F = dd.shape[0]
    EX = {16: 4, 4: 2}[n_ep]
    EY = n_ep // EX
    TZ = n_tp // 2
    S = CAP * n_ep
    S8 = PAD * n_ep
    Q = N // LANES
    PER = LANES // R
    RC = R * EX
    ey, ex = e // EX, lax.rem(e, EX)
    tz, tc = t // 2, lax.rem(t, 2)

    def at(index, size):
        return pl.ds(pl.multiple_of(index * size, size), size)

    def ring(d, n):
        return min(d, n - d)

    ep_far = sorted(range(1, n_ep), key=lambda k: -(ring(k // EX, EY) + ring(k % EX, EX)))
    tp_far = sorted(range(1, n_tp), key=lambda k: -(ring(k // 2, TZ) * 2 + k % 2))
    dy_far = sorted(range(EY), key=lambda d: -ring(d, EY))
    dx_far = sorted(range(EX), key=lambda d: -ring(d, EX))

    def ep_peer(k):
        return lax.rem(ey + k // EX, EY) * EX + lax.rem(ex + k % EX, EX)

    def tp_peer(k):
        return lax.rem(tz + k // 2, TZ) * 2 + lax.rem(tc + k % 2, 2)

    loads = []

    def load(src, dst):
        copy = pltpu.make_async_copy(src, dst, load_sems.at[len(loads)])
        copy.start()
        loads.append(copy)
        return copy

    pending = []

    def ep_start(phase, k, src, dst):
        copy = pltpu.make_async_remote_copy(
            src_ref=src,
            dst_ref=dst,
            send_sem=send_ep.at[phase, k],
            recv_sem=recv_ep.at[phase, k],
            device_id={"ep": ep_peer(k)},
            device_id_type=MESH,
        )
        copy.start()
        pending.append(copy)
        return copy

    def tp_start(phase, k, src, dst):
        copy = pltpu.make_async_remote_copy(
            src_ref=src,
            dst_ref=dst,
            send_sem=send_tp.at[phase, k],
            recv_sem=recv_tp.at[phase, k],
            device_id={"tp": tp_peer(k)},
            device_id_type=MESH,
        )
        copy.start()
        pending.append(copy)
        return copy

    def cross(phase, src, dst):
        return pltpu.make_async_remote_copy(
            src_ref=src,
            dst_ref=dst,
            send_sem=send_tr.at[phase],
            recv_sem=recv_tr.at[phase],
            device_id={"ep": t, "tp": e},
            device_id_type=MESH,
        )

    barrier = pltpu.get_barrier_semaphore()
    for k in ep_far:
        pl.semaphore_signal(barrier, inc=1, device_id={"ep": ep_peer(k)}, device_id_type=MESH)
    for k in tp_far:
        pl.semaphore_signal(barrier, inc=1, device_id={"tp": tp_peer(k)}, device_id_type=MESH)

    load_w = [
        load(src, wcat.at[:, pl.ds(i * W, W)])
        for i, src in enumerate((wq_hbm, wk_hbm, wv_hbm, wo_hbm))
    ]
    load_proj = load(wproj_hbm, wproj.at[at(t, W), :])
    load_state = load(state_hbm, state)
    load_dg, load_du = load(dg_hbm, dgu.at[:, pl.ds(0, F)]), load(du_hbm, dgu.at[:, pl.ds(F, F)])
    load_eg, load_eu = load(eg_hbm, eg), load(eu_hbm, eu)
    load_ed, load_dd = load(ed_hbm, ed), load(dd_hbm, dd)

    wide = tokens_ref[...].astype(F32)
    scale = lax.rsqrt(jnp.mean(wide * wide, axis=-1, keepdims=True) + EPS)
    nrm[...] = (wide * scale * gain_ref[...]).astype(BF16)

    r0, r1 = routes_ref[0:1, :], routes_ref[1:2, :]
    w0, w1 = weight_ref[0:1, :], weight_ref[1:2, :]
    total = w0 + w1
    which = iota((n_ep, R), 0)
    hit0, hit1 = which == r0, which == r1
    named = jnp.where(jnp.logical_or(hit0, hit1), 1.0, 0.0)
    earlier = jnp.where(iota((R, R), 0) < iota((R, R), 1), 1.0, 0.0).astype(BF16)
    slot = dot(named.astype(BF16), earlier)
    code = jnp.where(named > 0.0, slot + 1.0, 0.0)
    group_at = (e * CAP).astype(F32)
    rowcode = jnp.where(named > 0.0, slot + (1.0 + group_at), 0.0)
    shares = jnp.where(hit0, w0 / total, 0.0) + jnp.where(hit1, w1 / total, 0.0)
    info[:, 0:R] = rowcode
    info[:, R : 2 * R] = shares
    info[:, 2 * R : LANES] = jnp.zeros((n_ep, LANES - 2 * R), F32)

    pl.semaphore_wait(barrier, n_ep - 1 + n_tp - 1)
    got_x = {k: ep_start(0, k, nrm.at[:, at(ep_peer(k), Dc)], x_all.at[at(e, R), :]) for k in ep_far}
    x_all[at(e, R), :] = nrm[:, at(e, Dc)]
    load_proj.wait()
    got_wp = {
        k: tp_start(0, k, wproj.at[at(t, W), :], wproj.at[at(t, W), :]) for k in tp_far
    }

    gate_in = dot_t(nrm[...], win_ref[...])
    gate_fo = dot_t(nrm[...], wfo_ref[...]) + bias_ref[...]
    mine = iota(gate_in.shape, 1) == t
    g_in = jnp.sum(jnp.where(mine, gate_in, 0.0), axis=1, keepdims=True)
    g_fo = jnp.sum(jnp.where(mine, gate_fo, 0.0), axis=1, keepdims=True)
    eye = iota((R, R), 0) == iota((R, R), 1)
    smax = jnp.sum(jnp.where(eye, smax_ref[...], 0.0), axis=1, keepdims=True)
    log_keep = jnp.minimum(g_fo, 0.0) - jnp.log(1.0 + jnp.exp(-jnp.abs(g_fo)))
    carried = log_keep + smax
    new_max = jnp.maximum(carried, g_in)
    keep = jnp.exp(carried - new_max)
    write = jnp.exp(g_in - new_max)
    max_out_ref[...] = jnp.sum(jnp.where(eye, new_max, 0.0), axis=0, keepdims=True)
    keep_ref[...] = jnp.broadcast_to(keep, keep_ref.shape)

    for copy in load_w:
        copy.wait()
    got_part = {}
    for dy in [(EY - d) % EY for d in range(EY)]:
        back = (EY - dy) % EY
        for dx in range(EX):
            k = dy * EX + dx
            if k:
                got_x[k].wait_recv()
        rows = at(lax.rem(ey + back, EY), RC)
        part_send[rows, :] = dot(x_all[rows, :], wcat[...]).astype(BF16)
        for dx in dx_far:
            k = back * EX + dx
            if k:
                got_part[k] = ep_start(1, k, part_send.at[at(ep_peer(k), R), :], part_recv.at[k])
    got_info = {k: ep_start(2, k, info, info_recv.at[k]) for k in ep_far}

    @pl.when(e != t)
    def _():
        cross(0, tokens_ref.at[:, at(t, Dc)], raw_blk).start()

    @pl.when(e == t)
    def _():
        raw_blk[...] = tokens_ref[:, at(t, Dc)]

    proj = part_send[at(e, R), :].astype(F32)
    for k in reversed(ep_far):
        got_part[k].wait_recv()
        proj += part_recv[k].astype(F32)

    load_state.wait()
    q = proj[:, 0:W]
    key = proj[:, W : 2 * W] * W ** (-0.5)
    val = proj[:, 2 * W : 3 * W]
    og = proj[:, 3 * W : 4 * W]
    key_w = write * key
    new_norm = keep * norm_ref[...] + key_w
    q_t = q.T
    for b in range(R):
        numer[b : b + 1, :] = jnp.sum(q_t[:, b : b + 1] * state[b, 0], axis=0, keepdims=True)
    top = keep * numer[...] + jnp.sum(q * key_w, axis=1, keepdims=True) * val
    denom = jnp.sum(q * new_norm, axis=1, keepdims=True)
    cell = top / jnp.maximum(jnp.abs(denom), 1.0)
    mix_send[...] = (cell / (1.0 + jnp.exp(-og))).astype(BF16)

    def mix_copy(k):
        return pltpu.make_async_remote_copy(
            src_ref=mix_send,
            dst_ref=mix_all.at[:, at(t, W)],
            send_sem=send_mx.at[k],
            recv_sem=recv_mx.at[t],
            device_id={"ep": ep_peer(k), "tp": e},
            device_id_type=MESH,
        )

    for k in ep_far:
        mix_copy(k).start()

    @pl.when(e != t)
    def _():
        mix_copy(0).start()

    @pl.when(e == t)
    def _():
        mix_all[:, at(t, W)] = mix_send[...]

    norm_out_ref[...] = new_norm
    keyw_ref[...] = key_w
    value_ref[...] = val

    for k in ep_far:
        got_info[k].wait_recv()
    quarter = iota((n_ep, LANES), 1) // R
    codes, sharesl = [], []

    info_recv[0] = info[...]
    for qq in range(Q):
        ctile = jnp.zeros((n_ep, LANES), F32)
        stile = jnp.zeros((n_ep, LANES), F32)
        for j in range(PER):
            g = qq * PER + j
            gy, gx = g // EX, g % EX
            slot_k = lax.rem(ey + (EY - gy), EY) * EX + lax.rem(ex + (EX - gx), EX)
            tile = info_recv[slot_k]
            there = quarter == j
            ctile += jnp.where(there, tile if j == 0 else pltpu.roll(tile, j * R, 1), 0.0)
            back = (j - 1) % PER * R
            stile += jnp.where(there, tile if back == 0 else pltpu.roll(tile, back, 1), 0.0)
        codes.append(ctile)
        sharesl.append(stile)
    code_all = jnp.concatenate(codes, axis=1) if Q > 1 else codes[0]
    share_all = jnp.concatenate(sharesl, axis=1) if Q > 1 else sharesl[0]
    row_no = (iota((S, N), 0) + 1).astype(F32)
    for p in range(n_ep):
        gmat[p * S : (p + 1) * S, :] = jnp.where(row_no == code_all[p : p + 1, :], 1.0, 0.0).astype(
            BF16
        )
    is_mine = iota((n_ep, N), 0) == e
    my_code = jnp.sum(jnp.where(is_mine, code_all, 0.0), axis=0, keepdims=True)
    my_share = jnp.sum(jnp.where(is_mine, share_all, 0.0), axis=0, keepdims=True)
    my_code8 = jnp.where(
        my_code > 0.0, my_code + ((PAD - CAP) * (iota((1, N), 1) // R)).astype(F32), 0.0
    )
    row_share = jnp.sum(
        jnp.where((iota((S8, N), 0) + 1).astype(F32) == my_code8, my_share, 0.0),
        axis=1,
        keepdims=True,
    )
    spread = jnp.where(
        jnp.logical_and(
            iota((S8, S), 0) // PAD * CAP + iota((S8, S), 0) % PAD == iota((S8, S), 1),
            iota((S8, S), 0) % PAD < CAP,
        ),
        1.0,
        0.0,
    ).astype(BF16)
    repeat = jnp.where(iota((S8, n_ep), 0) // PAD == iota((S8, n_ep), 1), 1.0, 0.0).astype(BF16)
    code_rep = dot(repeat, code.astype(BF16))
    pick_t = jnp.where((iota((S8, R), 0) % PAD + 1).astype(F32) == code_rep, 1.0, 0.0)
    pick = pick_t.T.astype(BF16)

    for k in tp_far:
        got_wp[k].wait_recv()

    @pl.when(e != t)
    def _():
        cross(0, tokens_ref.at[:, at(t, Dc)], raw_blk).wait()

    for tt in range(n_tp):

        @pl.when(jnp.logical_or(e != t, t != tt))
        def _():
            pltpu.make_async_remote_copy(
                src_ref=mix_send,
                dst_ref=mix_all.at[:, pl.ds(tt * W, W)],
                send_sem=send_mx.at[0],
                recv_sem=recv_mx.at[tt],
                device_id={"ep": t, "tp": e},
                device_id_type=MESH,
            ).wait_recv()

    mine_res = raw_blk[...].astype(F32) + dot(mix_all[...], wproj[...])
    res_all[at(t, R), :] = mine_res.astype(BF16)
    got_res = {
        k: tp_start(1, k, res_all.at[at(t, R), :], res_all.at[at(t, R), :]) for k in tp_far
    }

    @pl.when(e != t)
    def _():
        cross(1, res_all.at[at(t, R), :], res_t).start()

    @pl.when(e == t)
    def _():
        res_t[...] = res_all[at(t, R), :]

    load_dg.wait()
    load_du.wait()
    my_fgain = fgain_ref[:, at(e, Dc)]
    wide_branch = branch_ref[...].astype(F32)
    pieces = Dc // LANES
    branch_rows = [
        jnp.sum(
            jnp.where(iota(wide_branch.shape, 0) == e * pieces + i, wide_branch, 0.0),
            axis=0,
            keepdims=True,
        )
        for i in range(pieces)
    ]
    my_branch = jnp.concatenate(branch_rows, axis=1) if pieces > 1 else branch_rows[0]
    my_branch = jnp.broadcast_to(my_branch, (8, Dc)).astype(BF16)
    ones = jnp.ones((8, Dc), BF16)

    for k in reversed(tp_far):
        got_res[k].wait_recv()
    block = res_all[...].astype(F32)
    xg[...] = (block * my_fgain).astype(BF16)
    square = block * block
    high = square.astype(BF16)
    low = (square - high.astype(F32)).astype(BF16)
    sums = dot_t(ones, high) + dot_t(ones, low)
    branch = dot_t(my_branch, xg[...])
    row8 = iota((8, LANES), 0)
    tile = jnp.zeros((8, LANES), F32)
    for qq in range(Q):
        cols = slice(qq * LANES, (qq + 1) * LANES)
        tile += jnp.where(row8 == qq, sums[:, cols], 0.0)
        tile += jnp.where(row8 == 4 + qq, branch[:, cols], 0.0)
    stat[...] = tile
    got_stat = {k: ep_start(3, k, stat, stat_recv.at[k]) for k in ep_far}

    got_dense = {}
    for dy in dy_far:
        rows = at(lax.rem(ey + dy, EY), RC)
        dense_send[rows, :] = dot(xg[rows, :], dgu[...]).astype(BF16)
        for dx in dx_far:
            k = dy * EX + dx
            if k:
                got_dense[k] = ep_start(
                    4, k, dense_send.at[at(ep_peer(k), R), :], dense_recv.at[k]
                )
    got_disp = {}
    for dy in dy_far:
        rows = at(lax.rem(ey + dy, EY), S * EX)
        disp_send[rows, :] = dot(gmat[rows, :], xg[...]).astype(BF16)
        for dx in dx_far:
            k = dy * EX + dx
            if k:
                got_disp[k] = ep_start(
                    5, k, disp_send.at[at(ep_peer(k), S), :], xrecv.at[:, at(e, Dc)]
                )
    xrecv[:, at(e, Dc)] = disp_send[at(e, S), :]

    for k in reversed(ep_far):
        got_stat[k].wait_recv()
        tile += stat_recv[k]
    scale_l = lax.rsqrt(tile[0:Q, :] * (1.0 / D) + EPS)
    share_l = 1.0 / (1.0 + jnp.exp(-(scale_l * tile[4 : 4 + Q, :])))
    my_scale = jnp.zeros((R, 1), F32)
    my_bshare = jnp.zeros((R, 1), F32)
    for qq in range(Q):
        here = iota((R, LANES), 1) + qq * LANES == iota((R, LANES), 0) + e * R
        my_scale += jnp.sum(jnp.where(here, scale_l[qq : qq + 1, :], 0.0), axis=1, keepdims=True)
        my_bshare += jnp.sum(jnp.where(here, share_l[qq : qq + 1, :], 0.0), axis=1, keepdims=True)
    scale_row = (
        jnp.concatenate([scale_l[qq : qq + 1, :] for qq in range(Q)], axis=1) if Q > 1 else scale_l
    )
    row_scale = jnp.sum(jnp.where(row_no == my_code, scale_row, 0.0), axis=1, keepdims=True)

    both = dense_send[at(e, R), :].astype(F32)
    for k in reversed(ep_far):
        got_dense[k].wait_recv()
        both += dense_recv[k].astype(F32)
    both *= my_scale
    g, u = both[:, :F], both[:, F:]
    hid_all[at(e, R), :] = (g / (1.0 + jnp.exp(-g)) * u).astype(BF16)
    got_hid = {
        k: ep_start(6, k, hid_all.at[at(e, R), :], hid_all.at[at(e, R), :]) for k in ep_far
    }

    load_eg.wait()
    load_eu.wait()
    for k in reversed(ep_far):
        got_disp[k].wait_recv()
    gp = dot(xrecv[...], eg[0]) * row_scale
    up = dot(xrecv[...], eu[0]) * row_scale
    ehid = (gp / (1.0 + jnp.exp(-gp)) * up).astype(BF16)
    ehid8 = dot(spread, ehid).astype(BF16)
    load_ed.wait()
    step = min(512, D)
    for c in range(D // step):
        cols = slice(c * step, (c + 1) * step)
        y = dot(ehid8, ed[0, :, cols]) * row_share
        fin_send[:, :, cols] = y.reshape(n_ep, PAD, step).astype(BF16)
    got_fin = {k: ep_start(7, k, fin_send.at[ep_peer(k)], fin_recv.at[e]) for k in ep_far}
    fin_recv[e] = fin_send[e]

    load_dd.wait()
    for k in reversed(ep_far):
        got_hid[k].wait_recv()
    got_dn = {}
    for dy in dy_far:
        rows = at(lax.rem(ey + dy, EY), RC)
        dn_send[rows, :] = dot(hid_all[rows, :], dd[...]).astype(BF16)
        for dx in dx_far:
            k = dy * EX + dx
            if k:
                got_dn[k] = ep_start(
                    8, k, dn_send.at[at(ep_peer(k), R), :], dn_recv.at[:, at(e, Dc)]
                )
    dn_recv[:, at(e, Dc)] = dn_send[at(e, R), :]

    for k in reversed(ep_far):
        got_fin[k].wait_recv()
    for k in reversed(ep_far):
        got_dn[k].wait_recv()
    got_tp = {}
    for k in tp_far + [0]:
        cols = at(tp_peer(k), Dt)
        back = fin_recv[:, :, cols].astype(F32).reshape(S8, Dt).astype(BF16)
        piece = dot(pick, back) + my_bshare * dn_recv[:, cols].astype(F32)
        tp_send[:, cols] = piece.astype(BF16)
        if k:
            got_tp[k] = tp_start(2, k, tp_send.at[:, cols], tp_recv.at[k])

    @pl.when(e != t)
    def _():
        cross(1, res_all.at[at(t, R), :], res_t).wait()

    last = res_t[...].astype(F32) + tp_send[:, at(t, Dt)].astype(F32)
    for k in reversed(tp_far):
        got_tp[k].wait_recv()
        last += tp_recv[k].astype(F32)
    out_all[:, at(t, Dt)] = last.astype(BF16)
    got_out = [
        tp_start(3, k, out_all.at[:, at(t, Dt)], out_all.at[:, at(t, Dt)]) for k in tp_far
    ]
    for k in ep_far:
        mix_copy(k).wait_send()

    @pl.when(e != t)
    def _():
        mix_copy(0).wait_send()

    for copy in got_out:
        copy.wait_recv()
    out_ref[...] = out_all[...]
    for copy in pending:
        copy.wait_send()


def on_device(
    n_ep,
    n_tp,
    tokens,
    state_matrix,
    state_norm,
    state_max,
    mixer_gain,
    w_query,
    w_key,
    w_value,
    w_outgate,
    w_ingate,
    w_forget,
    forget_bias,
    w_proj,
    ffn_gain,
    w_branch,
    routes,
    route_weight,
    expert_gate,
    expert_up,
    expert_down,
    dense_gate,
    dense_up,
    dense_down,
):
    R, D = tokens.shape
    hd = state_norm.shape[2]
    N, Dc, Dt, W = R * n_ep, D // n_ep, D // n_tp, hd
    F = dense_gate.shape[1]
    FE = expert_gate.shape[2]
    S, S8 = CAP * n_ep, PAD * n_ep
    vmem = pl.BlockSpec(memory_space=pltpu.VMEM)
    hbm = pl.BlockSpec(memory_space=pl.ANY)
    V = pltpu.VMEM
    scratch = [
        V(state_matrix.shape, F32),
        V((Dc, 4 * W), BF16),
        V((n_tp * W, Dc), BF16),
        V(expert_gate.shape, BF16),
        V(expert_up.shape, BF16),
        V(expert_down.shape, BF16),
        V((Dc, 2 * F), BF16),
        V(dense_down.shape, BF16),
        V((R, D), BF16),
        V((N, Dc), BF16),
        V((n_ep, LANES), F32),
        V((n_ep, n_ep, LANES), F32),
        V((N, 4 * W), BF16),
        V((n_ep, R, 4 * W), BF16),
        V((R, W), F32),
        V((R, W), BF16),
        V((R, n_tp * W), BF16),
        V((R, Dc), BF16),
        V((N, Dc), BF16),
        V((R, Dt), BF16),
        V((N, Dc), BF16),
        V((n_ep * S, N), BF16),
        V((8, LANES), F32),
        V((n_ep, 8, LANES), F32),
        V((N, 2 * F), BF16),
        V((n_ep, R, 2 * F), BF16),
        V((n_ep * S, Dc), BF16),
        V((S, D), BF16),
        V((N, F), BF16),
        V((n_ep, PAD, D), BF16),
        V((n_ep, PAD, D), BF16),
        V((N, Dc), BF16),
        V((R, D), BF16),
        V((R, D), BF16),
        V((n_tp, R, Dt), BF16),
        V((R, D), BF16),
        pltpu.SemaphoreType.DMA((12,)),
        pltpu.SemaphoreType.DMA((9, n_ep)),
        pltpu.SemaphoreType.DMA((9, n_ep)),
        pltpu.SemaphoreType.DMA((4, n_tp)),
        pltpu.SemaphoreType.DMA((4, n_tp)),
        pltpu.SemaphoreType.DMA((n_ep,)),
        pltpu.SemaphoreType.DMA((n_tp,)),
        pltpu.SemaphoreType.DMA((2,)),
        pltpu.SemaphoreType.DMA((2,)),
    ]
    Sh = jax.ShapeDtypeStruct
    layer_out, new_norm, new_max, key_w, value, keep = pl.pallas_call(
        functools.partial(layer_kernel, n_ep, n_tp),
        out_shape=(
            Sh((R, D), BF16),
            Sh((R, hd), F32),
            Sh((1, R), F32),
            Sh((R, hd), F32),
            Sh((R, hd), F32),
            Sh((R, hd), F32),
        ),
        in_specs=[vmem] * 11 + [hbm] * 12,
        out_specs=(vmem,) * 6,
        scratch_shapes=scratch,
        compiler_params=pltpu.CompilerParams(
            collective_id=0, has_side_effects=True, vmem_limit_bytes=66_000_000
        ),
    )(
        tokens,
        mixer_gain[None, :],
        w_ingate.T,
        w_forget.T,
        forget_bias[None, :],
        state_norm.reshape(R, hd),
        state_max.T,
        ffn_gain[None, :],
        w_branch.reshape(-1, LANES),
        routes.T,
        route_weight.T,
        state_matrix,
        w_query,
        w_key,
        w_value,
        w_outgate,
        w_proj,
        expert_gate,
        expert_up,
        expert_down,
        dense_gate,
        dense_up,
        dense_down,
    )
    new_matrix = (
        keep[:, None, None, :] * state_matrix + key_w[:, None, :, None] * value[:, None, None, :]
    )
    return (layer_out, new_matrix, new_norm.reshape(R, 1, hd), new_max.T)


def solution(mesh):
    in_specs = (
        P("ep", None),
        P("ep", "tp", None, None),
        P("ep", "tp", None),
        P("ep", "tp"),
        P(),
        P("ep", "tp"),
        P("ep", "tp"),
        P("ep", "tp"),
        P("ep", "tp"),
        P(),
        P(),
        P(),
        P("tp", "ep"),
        P(),
        P(),
        P("ep", None),
        P("ep", None),
        P("ep", None, "tp"),
        P("ep", None, "tp"),
        P("ep", "tp", None),
        P("ep", "tp"),
        P("ep", "tp"),
        P("tp", "ep"),
    )
    out_specs = (P("ep", None), P("ep", "tp", None, None), P("ep", "tp", None), P("ep", "tp"))
    return jax.shard_map(
        functools.partial(on_device, mesh.shape["ep"], mesh.shape["tp"]),
        mesh=mesh,
        in_specs=in_specs,
        out_specs=out_specs,
        check_vma=False,
    )
```

time: 257 us -> 129 us (0.50)
  Pallas kernels: 241 us -> 123 us
  local copies, waits for them, and re-layouts: 9.22 us -> 1.83 us
    pallas_call x1, Pallas kernels: 241 us -> 123 us  [on_device(): pl.pallas_call(functools.partial(layer_kernel, n_ep, n_tp), out_shape=(Sh...]
    unnamed x10 -> x9, local copies, waits for them, and re-layouts: 6.67 us -> 1.83 us
where the time goes in v1:
time: 129 us
  Pallas kernels  123 us (95%)
  other arithmetic  2.96 us (2%)
  local copies, waits for them, and re-layouts  1.83 us (1%)
    pallas_call x1, Pallas kernels, on_device(): pl.pallas_call(functools.partial(layer_kernel, n_ep, n_tp), out_shape=(Sh...  123 us
    add x1, other arithmetic, on_device(): keep[:, None, None, :] * state_matrix  2.96 us

profile of v1, /device:TPU:1, one launch (start us, length us, event | category | flops | bytes accessed | tf_op | source)
XLA Modules:
  0.0 128.8 jit_solution(16028922037295204360)
XLA Ops:
  0.6 123.4 %shard_map.246 = (bf16[32,4096]{1,0:T(8,128)(2,1)}, f32[32,128]{1,0:T(8,128)}, f32[1,32]{1,0:T(1,128)}, f32[32,128]{1,0:T(8,128)}, f32[32,128]{1,0:T(8,128)}, /*index=5*/f32[32,128]{1,0:T(8,128)}) custom-call(bf16[32,4096]{1,0:T(8,128)(2,1)} %tokens_ref.1, f32[1,4096]{1,0:T(1,128)} %bitcast.16, bf16[16,4096]{1,0:T(8,128)(2,1)} %bitcast.14, ...), custom_call_target="tpu_custom_call" | custom-call | tf_op jit(solution)/shard_map/pallas_call | solution.py:644
  124.0 0.0 copy-start
  124.0 0.0 copy-start.1
  124.0 0.0 copy-start.2
  124.0 3.0 %multiply_add_fusion = f32[32,1,128,128]{3,2,1,0:T(8,128)} fusion(f32[32,1,128,128]{3,2,1,0:T(8,128)} %state_hbm.1, f32[32,128]{1,0:T(8,128)} %get-tuple-element.13, f32[32,128]{1,0:T(8,128)} %get-tuple-element.12, f32[32,128]{1,0:T(8,128)} %get-tuple-element.11), kind=kLoop, calls=%fused_computation | loop fusion | flops 1572864 | bytes 4243456 | tf_op jit(solution)/shard_map/add | solution.py:686
  127.0 0.0 copy-done
  127.0 0.7 copy.31
  127.7 0.0 copy-done.1
  127.7 0.6 copy.32
  128.3 0.0 copy-done.2
  128.3 0.5 copy.33
Async XLA Ops:
  124.0 3.0 %copy-start = (bf16[32,4096]{1,0:T(8,128)(2,1)S(1)}, bf16[32,4096]{1,0:T(8,128)(2,1)}, u32[]{:S(2)}) copy-start(bf16[32,4096]{1,0:T(8,128)(2,1)} %get-tuple-element.24) | copy-start | bytes 786436
  124.0 3.7 %copy-start.1 = (f32[32,128]{1,0:T(8,128)S(1)}, f32[32,128]{1,0:T(8,128)}, u32[]{:S(2)}) copy-start(f32[32,128]{1,0:T(8,128)} %get-tuple-element.14) | copy-start | bytes 49156
  124.0 4.3 %copy-start.2 = (f32[1,32]{1,0:T(1,128)S(1)}, f32[1,32]{1,0:T(1,128)}, u32[]{:S(2)}) copy-start(f32[1,32]{1,0:T(1,128)} %get-tuple-element.15) | copy-start | bytes 388

commit v2 on v1

--- a/solution.py
+++ b/solution.py
@@ -65,7 +65,7 @@
     wproj,
     eg,
     eu,
-    ed,
+    edc,
     dgu,
     dd,
     nrm,
@@ -89,8 +89,12 @@
     disp_send,
     xrecv,
     hid_all,
+    yo_send,
+    yo_recv,
     fin_send,
     fin_recv,
+    dno_send,
+    dno_recv,
     dn_send,
     dn_recv,
     tp_send,
@@ -105,13 +109,18 @@
     recv_mx,
     send_tr,
     recv_tr,
+    send_fw,
+    recv_fw,
+    send_sb,
+    recv_sb,
 ):
     e = lax.axis_index("ep")
     t = lax.axis_index("tp")
     R, D = tokens_ref.shape
     N = R * n_ep
     Dc = D // n_ep
-    Dt = D // n_tp
+    HD = Dc // 2
+    DH = D // 2
     W = mix_send.shape[1]
     F = dd.shape[0]
     EX = {16: 4, 4: 2}[n_ep]
@@ -132,15 +141,20 @@
         return min(d, n - d)
 
     ep_far = sorted(range(1, n_ep), key=lambda k: -(ring(k // EX, EY) + ring(k % EX, EX)))
-    tp_far = sorted(range(1, n_tp), key=lambda k: -(ring(k // 2, TZ) * 2 + k % 2))
+    dz_far = sorted(range(1, TZ), key=lambda d: -ring(d, TZ))
     dy_far = sorted(range(EY), key=lambda d: -ring(d, EY))
     dx_far = sorted(range(EX), key=lambda d: -ring(d, EX))
 
     def ep_peer(k):
         return lax.rem(ey + k // EX, EY) * EX + lax.rem(ex + k % EX, EX)
 
+    def ep_from(k):
+        return lax.rem(ey + EY - k // EX, EY) * EX + lax.rem(ex + EX - k % EX, EX)
+
     def tp_peer(k):
         return lax.rem(tz + k // 2, TZ) * 2 + lax.rem(tc + k % 2, 2)
+
+    sibling = tz * 2 + 1 - tc
 
     loads = []
 
@@ -178,6 +192,39 @@
         pending.append(copy)
         return copy
 
+    def side_start(send_sem, recv_sem, src, dst):
+        copy = pltpu.make_async_remote_copy(
+            src_ref=src,
+            dst_ref=dst,
+            send_sem=send_sem,
+            recv_sem=recv_sem,
+            device_id={"tp": sibling},
+            device_id_type=MESH,
+        )
+        copy.start()
+        pending.append(copy)
+        return copy
+
+    def spread_tp(phase, region):
+        copies = {dz: tp_start(phase, 2 * dz, region(t), region(t)) for dz in dz_far}
+        copies[0] = tp_start(phase, 1, region(t), region(t))
+        return copies
+
+    def gather_tp(phase, region, copies):
+        passed = []
+        for dz in reversed(dz_far):
+            copies[dz].wait_recv()
+            source = lax.rem(tz + TZ - dz, TZ) * 2 + tc
+            odd = 2 * dz + 1
+            passed.append(
+                side_start(
+                    send_tp.at[phase, odd], recv_tp.at[phase, odd], region(source), region(source)
+                )
+            )
+        copies[0].wait_recv()
+        for copy in passed:
+            copy.wait_recv()
+
     def cross(phase, src, dst):
         return pltpu.make_async_remote_copy(
             src_ref=src,
@@ -191,7 +238,7 @@
     barrier = pltpu.get_barrier_semaphore()
     for k in ep_far:
         pl.semaphore_signal(barrier, inc=1, device_id={"ep": ep_peer(k)}, device_id_type=MESH)
-    for k in tp_far:
+    for k in range(1, n_tp):
         pl.semaphore_signal(barrier, inc=1, device_id={"tp": tp_peer(k)}, device_id_type=MESH)
 
     load_w = [
@@ -202,7 +249,12 @@
     load_state = load(state_hbm, state)
     load_dg, load_du = load(dg_hbm, dgu.at[:, pl.ds(0, F)]), load(du_hbm, dgu.at[:, pl.ds(F, F)])
     load_eg, load_eu = load(eg_hbm, eg), load(eu_hbm, eu)
-    load_ed, load_dd = load(ed_hbm, ed), load(dd_hbm, dd)
+    load_ed = [
+        load(ed_hbm.at[0, :, at(2 * b + side, HD)], edc.at[i, :, pl.ds(b * HD, HD)])
+        for i, side in enumerate((1 - tc, tc))
+        for b in range(n_ep)
+    ]
+    load_dd = load(dd_hbm, dd)
 
     wide = tokens_ref[...].astype(F32)
     scale = lax.rsqrt(jnp.mean(wide * wide, axis=-1, keepdims=True) + EPS)
@@ -228,9 +280,11 @@
     got_x = {k: ep_start(0, k, nrm.at[:, at(ep_peer(k), Dc)], x_all.at[at(e, R), :]) for k in ep_far}
     x_all[at(e, R), :] = nrm[:, at(e, Dc)]
     load_proj.wait()
-    got_wp = {
-        k: tp_start(0, k, wproj.at[at(t, W), :], wproj.at[at(t, W), :]) for k in tp_far
-    }
+
+    def proj_rows(tt):
+        return wproj.at[at(tt, W), :]
+
+    got_wp = spread_tp(0, proj_rows)
 
     gate_in = dot_t(nrm[...], win_ref[...])
     gate_fo = dot_t(nrm[...], wfo_ref[...]) + bias_ref[...]
@@ -313,6 +367,7 @@
     def _():
         mix_all[:, at(t, W)] = mix_send[...]
 
+    gather_tp(0, proj_rows, got_wp)
     norm_out_ref[...] = new_norm
     keyw_ref[...] = key_w
     value_ref[...] = val
@@ -368,9 +423,6 @@
     pick_t = jnp.where((iota((S8, R), 0) % PAD + 1).astype(F32) == code_rep, 1.0, 0.0)
     pick = pick_t.T.astype(BF16)
 
-    for k in tp_far:
-        got_wp[k].wait_recv()
-
     @pl.when(e != t)
     def _():
         cross(0, tokens_ref.at[:, at(t, Dc)], raw_blk).wait()
@@ -390,17 +442,32 @@
 
     mine_res = raw_blk[...].astype(F32) + dot(mix_all[...], wproj[...])
     res_all[at(t, R), :] = mine_res.astype(BF16)
-    got_res = {
-        k: tp_start(1, k, res_all.at[at(t, R), :], res_all.at[at(t, R), :]) for k in tp_far
-    }
-
-    @pl.when(e != t)
-    def _():
-        cross(1, res_all.at[at(t, R), :], res_t).start()
-
-    @pl.when(e == t)
-    def _():
-        res_t[...] = res_all[at(t, R), :]
+
+    def res_rows(tt):
+        return res_all.at[at(tt, R), :]
+
+    got_res = spread_tp(1, res_rows)
+
+    def half_copy(c):
+        return pltpu.make_async_remote_copy(
+            src_ref=res_all.at[at(t, R), pl.ds(c * HD, HD)],
+            dst_ref=res_t.at[:, at(lax.rem(e, 2), HD)],
+            send_sem=send_tr.at[1 + c],
+            recv_sem=recv_tr.at[1 + lax.rem(e, 2)],
+            device_id={"ep": t, "tp": e // 2 * 2 + c},
+            device_id_type=MESH,
+        )
+
+    for c in range(2):
+        away = jnp.logical_or(e != t, tc != c)
+
+        @pl.when(away)
+        def _():
+            half_copy(c).start()
+
+        @pl.when(jnp.logical_not(away))
+        def _():
+            res_t[:, pl.ds(c * HD, HD)] = res_all[at(t, R), pl.ds(c * HD, HD)]
 
     load_dg.wait()
     load_du.wait()
@@ -419,8 +486,7 @@
     my_branch = jnp.broadcast_to(my_branch, (8, Dc)).astype(BF16)
     ones = jnp.ones((8, Dc), BF16)
 
-    for k in reversed(tp_far):
-        got_res[k].wait_recv()
+    gather_tp(1, res_rows, got_res)
     block = res_all[...].astype(F32)
     xg[...] = (block * my_fgain).astype(BF16)
     square = block * block
@@ -450,14 +516,20 @@
     got_disp = {}
     for dy in dy_far:
         rows = at(lax.rem(ey + dy, EY), S * EX)
-        disp_send[rows, :] = dot(gmat[rows, :], xg[...]).astype(BF16)
+        disp_send[rows, :] = dot(gmat[rows, :], xg[:, at(tc, HD)]).astype(BF16)
         for dx in dx_far:
             k = dy * EX + dx
             if k:
                 got_disp[k] = ep_start(
-                    5, k, disp_send.at[at(ep_peer(k), S), :], xrecv.at[:, at(e, Dc)]
+                    5, k, disp_send.at[at(ep_peer(k), S), :], xrecv.at[:, at(2 * e + tc, HD)]
                 )
-    xrecv[:, at(e, Dc)] = disp_send[at(e, S), :]
+    xrecv[:, at(2 * e + tc, HD)] = disp_send[at(e, S), :]
+
+    def forward(k):
+        region = xrecv.at[:, at(2 * ep_from(k) + tc, HD)]
+        return side_start(send_fw.at[k], recv_fw.at[k], region, region)
+
+    passed = [forward(0)]
 
     for k in reversed(ep_far):
         got_stat[k].wait_recv()
@@ -490,15 +562,27 @@
     load_eu.wait()
     for k in reversed(ep_far):
         got_disp[k].wait_recv()
+        passed.append(forward(k))
+    for copy in passed:
+        copy.wait_recv()
     gp = dot(xrecv[...], eg[0]) * row_scale
     up = dot(xrecv[...], eu[0]) * row_scale
     ehid = (gp / (1.0 + jnp.exp(-gp)) * up).astype(BF16)
     ehid8 = dot(spread, ehid).astype(BF16)
-    load_ed.wait()
-    step = min(512, D)
-    for c in range(D // step):
-        cols = slice(c * step, (c + 1) * step)
-        y = dot(ehid8, ed[0, :, cols]) * row_share
+    for copy in load_ed:
+        copy.wait()
+    step = min(512, DH)
+    strips = [slice(c * step, (c + 1) * step) for c in range(DH // step)]
+    got_yo = []
+    for i, cols in enumerate(strips):
+        yo_send[:, cols] = (dot(ehid8, edc[0, :, cols]) * row_share).astype(BF16)
+        got_yo.append(
+            side_start(send_sb.at[i], recv_sb.at[i], yo_send.at[:, cols], yo_recv.at[:, cols])
+        )
+    for copy, cols in zip(got_yo, strips):
+        y = dot(ehid8, edc[1, :, cols]) * row_share
+        copy.wait_recv()
+        y += yo_recv[:, cols].astype(F32)
         fin_send[:, :, cols] = y.reshape(n_ep, PAD, step).astype(BF16)
     got_fin = {k: ep_start(7, k, fin_send.at[ep_peer(k)], fin_recv.at[e]) for k in ep_far}
     fin_recv[e] = fin_send[e]
@@ -506,43 +590,63 @@
     load_dd.wait()
     for k in reversed(ep_far):
         got_hid[k].wait_recv()
+    got_no = {}
+    for dy in dy_far:
+        rows = at(lax.rem(ey + dy, EY), RC)
+        dno_send[rows, :] = dot(hid_all[rows, :], dd[:, at(1 - tc, HD)]).astype(BF16)
+        got_no[dy] = side_start(
+            send_sb.at[4 + dy], recv_sb.at[4 + dy], dno_send.at[rows, :], dno_recv.at[rows, :]
+        )
     got_dn = {}
     for dy in dy_far:
         rows = at(lax.rem(ey + dy, EY), RC)
-        dn_send[rows, :] = dot(hid_all[rows, :], dd[...]).astype(BF16)
+        down = dot(hid_all[rows, :], dd[:, at(tc, HD)])
+        got_no[dy].wait_recv()
+        dn_send[rows, :] = (down + dno_recv[rows, :].astype(F32)).astype(BF16)
         for dx in dx_far:
             k = dy * EX + dx
             if k:
                 got_dn[k] = ep_start(
-                    8, k, dn_send.at[at(ep_peer(k), R), :], dn_recv.at[:, at(e, Dc)]
+                    8, k, dn_send.at[at(ep_peer(k), R), :], dn_recv.at[:, at(e, HD)]
                 )
-    dn_recv[:, at(e, Dc)] = dn_send[at(e, R), :]
+    dn_recv[:, at(e, HD)] = dn_send[at(e, R), :]
 
     for k in reversed(ep_far):
         got_fin[k].wait_recv()
     for k in reversed(ep_far):
         got_dn[k].wait_recv()
     got_tp = {}
-    for k in tp_far + [0]:
-        cols = at(tp_peer(k), Dt)
-        back = fin_recv[:, :, cols].astype(F32).reshape(S8, Dt).astype(BF16)
+    for dz in dz_far + [0]:
+        cols = at(lax.rem(tz + dz, TZ), Dc)
+        back = fin_recv[:, :, cols].astype(F32).reshape(S8, Dc).astype(BF16)
         piece = dot(pick, back) + my_bshare * dn_recv[:, cols].astype(F32)
         tp_send[:, cols] = piece.astype(BF16)
-        if k:
-            got_tp[k] = tp_start(2, k, tp_send.at[:, cols], tp_recv.at[k])
-
-    @pl.when(e != t)
-    def _():
-        cross(1, res_all.at[at(t, R), :], res_t).wait()
-
-    last = res_t[...].astype(F32) + tp_send[:, at(t, Dt)].astype(F32)
-    for k in reversed(tp_far):
-        got_tp[k].wait_recv()
-        last += tp_recv[k].astype(F32)
-    out_all[:, at(t, Dt)] = last.astype(BF16)
-    got_out = [
-        tp_start(3, k, out_all.at[:, at(t, Dt)], out_all.at[:, at(t, Dt)]) for k in tp_far
-    ]
+        if dz:
+            got_tp[dz] = tp_start(2, 2 * dz, tp_send.at[:, cols], tp_recv.at[dz])
+
+    for i in range(2):
+
+        @pl.when(jnp.logical_or(e != t, lax.rem(e, 2) != i))
+        def _():
+            pltpu.make_async_remote_copy(
+                src_ref=res_all.at[at(t, R), pl.ds(0, HD)],
+                dst_ref=res_t.at[:, pl.ds(i * HD, HD)],
+                send_sem=send_tr.at[1 + i],
+                recv_sem=recv_tr.at[1 + i],
+                device_id={"ep": t, "tp": e},
+                device_id_type=MESH,
+            ).wait_recv()
+
+    last = res_t[...].astype(F32) + tp_send[:, at(tz, Dc)].astype(F32)
+    for dz in reversed(dz_far):
+        got_tp[dz].wait_recv()
+        last += tp_recv[dz].astype(F32)
+    out_all[:, at(tc * TZ + tz, Dc)] = last.astype(BF16)
+
+    def out_cols(tt):
+        return out_all.at[:, at(lax.rem(tt, 2) * TZ + tt // 2, Dc)]
+
+    got_out = spread_tp(3, out_cols)
     for k in ep_far:
         mix_copy(k).wait_send()
 
@@ -550,9 +654,16 @@
     def _():
         mix_copy(0).wait_send()
 
-    for copy in got_out:
-        copy.wait_recv()
-    out_ref[...] = out_all[...]
+    for c in range(2):
+
+        @pl.when(jnp.logical_or(e != t, tc != c))
+        def _():
+            half_copy(c).wait_send()
+
+    gather_tp(3, out_cols, got_out)
+    for b in range(n_ep):
+        for c in range(2):
+            out_ref[:, pl.ds((2 * b + c) * HD, HD)] = out_all[:, pl.ds(c * DH + b * HD, HD)]
     for copy in pending:
         copy.wait_send()
 
@@ -586,7 +697,7 @@
 ):
     R, D = tokens.shape
     hd = state_norm.shape[2]
-    N, Dc, Dt, W = R * n_ep, D // n_ep, D // n_tp, hd
+    N, Dc, DH, W = R * n_ep, D // n_ep, D // 2, hd
     F = dense_gate.shape[1]
     FE = expert_gate.shape[2]
     S, S8 = CAP * n_ep, PAD * n_ep
@@ -599,7 +710,7 @@
         V((n_tp * W, Dc), BF16),
         V(expert_gate.shape, BF16),
         V(expert_up.shape, BF16),
-        V(expert_down.shape, BF16),
+        V((2, FE, DH), BF16),
         V((Dc, 2 * F), BF16),
         V(dense_down.shape, BF16),
         V((R, D), BF16),
@@ -613,32 +724,40 @@
         V((R, n_tp * W), BF16),
         V((R, Dc), BF16),
         V((N, Dc), BF16),
-        V((R, Dt), BF16),
+        V((R, Dc), BF16),
         V((N, Dc), BF16),
         V((n_ep * S, N), BF16),
         V((8, LANES), F32),
         V((n_ep, 8, LANES), F32),
         V((N, 2 * F), BF16),
         V((n_ep, R, 2 * F), BF16),
-        V((n_ep * S, Dc), BF16),
+        V((n_ep * S, Dc // 2), BF16),
         V((S, D), BF16),
         V((N, F), BF16),
-        V((n_ep, PAD, D), BF16),
-        V((n_ep, PAD, D), BF16),
-        V((N, Dc), BF16),
+        V((S8, DH), BF16),
+        V((S8, DH), BF16),
+        V((n_ep, PAD, DH), BF16),
+        V((n_ep, PAD, DH), BF16),
+        V((N, Dc // 2), BF16),
+        V((N, Dc // 2), BF16),
+        V((N, Dc // 2), BF16),
+        V((R, DH), BF16),
+        V((R, DH), BF16),
+        V((n_tp // 2, R, Dc), BF16),
         V((R, D), BF16),
-        V((R, D), BF16),
-        V((n_tp, R, Dt), BF16),
-        V((R, D), BF16),
-        pltpu.SemaphoreType.DMA((12,)),
+        pltpu.SemaphoreType.DMA((11 + 2 * n_ep,)),
         pltpu.SemaphoreType.DMA((9, n_ep)),
         pltpu.SemaphoreType.DMA((9, n_ep)),
         pltpu.SemaphoreType.DMA((4, n_tp)),
         pltpu.SemaphoreType.DMA((4, n_tp)),
         pltpu.SemaphoreType.DMA((n_ep,)),
         pltpu.SemaphoreType.DMA((n_tp,)),
-        pltpu.SemaphoreType.DMA((2,)),
-        pltpu.SemaphoreType.DMA((2,)),
+        pltpu.SemaphoreType.DMA((3,)),
+        pltpu.SemaphoreType.DMA((3,)),
+        pltpu.SemaphoreType.DMA((n_ep,)),
+        pltpu.SemaphoreType.DMA((n_ep,)),
+        pltpu.SemaphoreType.DMA((8,)),
+        pltpu.SemaphoreType.DMA((8,)),
     ]
     Sh = jax.ShapeDtypeStruct
     layer_out, new_norm, new_max, key_w, value, keep = pl.pallas_call(

time: 129 us -> 106 us (0.82)
  Pallas kernels: 123 us -> 100 us
    pallas_call x1, Pallas kernels: 123 us -> 100 us  [on_device(): pl.pallas_call(functools.partial(layer_kernel, n_ep, n_tp), out_shape=(Sh...]
where the time goes in v2:
time: 106 us
  Pallas kernels  100 us (94%)
  other arithmetic  2.96 us (3%)
  local copies, waits for them, and re-layouts  1.83 us (2%)
    pallas_call x1, Pallas kernels, on_device(): pl.pallas_call(functools.partial(layer_kernel, n_ep, n_tp), out_shape=(Sh...  100 us
    add x1, other arithmetic, on_device(): keep[:, None, None, :] * state_matrix  2.96 us

profile of v2, /device:TPU:1, one launch (start us, length us, event | category | flops | bytes accessed | tf_op | source)
XLA Modules:
  0.0 105.9 jit_solution(11355043333273762921)
XLA Ops:
  0.6 100.5 %shard_map.246 = (bf16[32,4096]{1,0:T(8,128)(2,1)}, f32[32,128]{1,0:T(8,128)}, f32[1,32]{1,0:T(1,128)}, f32[32,128]{1,0:T(8,128)}, f32[32,128]{1,0:T(8,128)}, /*index=5*/f32[32,128]{1,0:T(8,128)}) custom-call(bf16[32,4096]{1,0:T(8,128)(2,1)} %tokens_ref.1, f32[1,4096]{1,0:T(1,128)} %bitcast.16, bf16[16,4096]{1,0:T(8,128)(2,1)} %bitcast.14, ...), custom_call_target="tpu_custom_call" | custom-call | tf_op jit(solution)/shard_map/pallas_call | solution.py:763
  101.1 0.0 copy-start
  101.1 0.0 copy-start.1
  101.1 0.0 copy-start.2
  101.1 3.0 %multiply_add_fusion = f32[32,1,128,128]{3,2,1,0:T(8,128)} fusion(f32[32,1,128,128]{3,2,1,0:T(8,128)} %state_hbm.1, f32[32,128]{1,0:T(8,128)} %get-tuple-element.13, f32[32,128]{1,0:T(8,128)} %get-tuple-element.12, f32[32,128]{1,0:T(8,128)} %get-tuple-element.11), kind=kLoop, calls=%fused_computation | loop fusion | flops 1572864 | bytes 4243456 | tf_op jit(solution)/shard_map/add | solution.py:805
  104.1 0.0 copy-done
  104.1 0.7 copy.31
  104.8 0.0 copy-done.1
  104.8 0.6 copy.32
  105.4 0.0 copy-done.2
  105.4 0.5 copy.33
Async XLA Ops:
  101.1 3.0 %copy-start = (bf16[32,4096]{1,0:T(8,128)(2,1)S(1)}, bf16[32,4096]{1,0:T(8,128)(2,1)}, u32[]{:S(2)}) copy-start(bf16[32,4096]{1,0:T(8,128)(2,1)} %get-tuple-element.24) | copy-start | bytes 786436
  101.1 3.7 %copy-start.1 = (f32[32,128]{1,0:T(8,128)S(1)}, f32[32,128]{1,0:T(8,128)}, u32[]{:S(2)}) copy-start(f32[32,128]{1,0:T(8,128)} %get-tuple-element.14) | copy-start | bytes 49156
  101.1 4.3 %copy-start.2 = (f32[1,32]{1,0:T(1,128)S(1)}, f32[1,32]{1,0:T(1,128)}, u32[]{:S(2)}) copy-start(f32[1,32]{1,0:T(1,128)} %get-tuple-element.15) | copy-start | bytes 388

commit v3 on v2

--- a/solution.py
+++ b/solution.py
@@ -85,7 +85,12 @@
     stat,
     stat_recv,
     dense_send,
-    dense_recv,
+    da_recv,
+    db_recv,
+    a2_send,
+    a2_recv,
+    b2_send,
+    b2_recv,
     disp_send,
     xrecv,
     hid_all,
@@ -113,6 +118,10 @@
     recv_fw,
     send_sb,
     recv_sb,
+    send_a,
+    recv_a,
+    send_b,
+    recv_b,
 ):
     e = lax.axis_index("ep")
     t = lax.axis_index("tp")
@@ -132,6 +141,7 @@
     PER = LANES // R
     RC = R * EX
     ey, ex = e // EX, lax.rem(e, EX)
+    mine_group = lax.rem(t + e, n_ep)
     tz, tc = t // 2, lax.rem(t, 2)
 
     def at(index, size):
@@ -225,15 +235,18 @@
         for copy in passed:
             copy.wait_recv()
 
-    def cross(phase, src, dst):
+    def raw_copy():
         return pltpu.make_async_remote_copy(
-            src_ref=src,
-            dst_ref=dst,
-            send_sem=send_tr.at[phase],
-            recv_sem=recv_tr.at[phase],
-            device_id={"ep": t, "tp": e},
+            src_ref=tokens_ref.at[:, at(t, Dc)],
+            dst_ref=raw_blk,
+            send_sem=send_tr.at[0],
+            recv_sem=recv_tr.at[0],
+            device_id={"ep": t, "tp": lax.rem(e + n_ep - t, n_ep)},
             device_id_type=MESH,
         )
+
+    raw_away = jnp.logical_or(e != 0, t != 0)
+    fin_recv[...] = jnp.zeros_like(fin_recv)
 
     barrier = pltpu.get_barrier_semaphore()
     for k in ep_far:
@@ -318,11 +331,11 @@
                 got_part[k] = ep_start(1, k, part_send.at[at(ep_peer(k), R), :], part_recv.at[k])
     got_info = {k: ep_start(2, k, info, info_recv.at[k]) for k in ep_far}
 
-    @pl.when(e != t)
+    @pl.when(raw_away)
     def _():
-        cross(0, tokens_ref.at[:, at(t, Dc)], raw_blk).start()
-
-    @pl.when(e == t)
+        raw_copy().start()
+
+    @pl.when(jnp.logical_not(raw_away))
     def _():
         raw_blk[...] = tokens_ref[:, at(t, Dc)]
 
@@ -352,18 +365,18 @@
             dst_ref=mix_all.at[:, at(t, W)],
             send_sem=send_mx.at[k],
             recv_sem=recv_mx.at[t],
-            device_id={"ep": ep_peer(k), "tp": e},
+            device_id={"ep": ep_peer(k), "tp": lax.rem(e + n_ep - ep_peer(k), n_ep)},
             device_id_type=MESH,
         )
 
     for k in ep_far:
         mix_copy(k).start()
 
-    @pl.when(e != t)
+    @pl.when(t != 0)
     def _():
         mix_copy(0).start()
 
-    @pl.when(e == t)
+    @pl.when(t == 0)
     def _():
         mix_all[:, at(t, W)] = mix_send[...]
 
@@ -423,55 +436,119 @@
     pick_t = jnp.where((iota((S8, R), 0) % PAD + 1).astype(F32) == code_rep, 1.0, 0.0)
     pick = pick_t.T.astype(BF16)
 
-    @pl.when(e != t)
+    @pl.when(raw_away)
     def _():
-        cross(0, tokens_ref.at[:, at(t, Dc)], raw_blk).wait()
+        raw_copy().wait()
 
     for tt in range(n_tp):
 
-        @pl.when(jnp.logical_or(e != t, t != tt))
-        def _():
+        def arrive_mix(tt=tt):
             pltpu.make_async_remote_copy(
                 src_ref=mix_send,
                 dst_ref=mix_all.at[:, pl.ds(tt * W, W)],
                 send_sem=send_mx.at[0],
                 recv_sem=recv_mx.at[tt],
-                device_id={"ep": t, "tp": e},
+                device_id={"tp": sibling},
                 device_id_type=MESH,
             ).wait_recv()
 
+        if tt:
+            arrive_mix()
+        else:
+            pl.when(t != 0)(arrive_mix)
+
     mine_res = raw_blk[...].astype(F32) + dot(mix_all[...], wproj[...])
-    res_all[at(t, R), :] = mine_res.astype(BF16)
+    my_rows = at(mine_group, R)
+    res_all[my_rows, :] = mine_res.astype(BF16)
 
     def res_rows(tt):
-        return res_all.at[at(tt, R), :]
+        return res_all.at[at(lax.rem(tt + e, n_ep), R), :]
 
     got_res = spread_tp(1, res_rows)
 
     def half_copy(c):
         return pltpu.make_async_remote_copy(
-            src_ref=res_all.at[at(t, R), pl.ds(c * HD, HD)],
+            src_ref=res_all.at[my_rows, pl.ds(c * HD, HD)],
             dst_ref=res_t.at[:, at(lax.rem(e, 2), HD)],
             send_sem=send_tr.at[1 + c],
             recv_sem=recv_tr.at[1 + lax.rem(e, 2)],
-            device_id={"ep": t, "tp": e // 2 * 2 + c},
+            device_id={"ep": mine_group, "tp": e // 2 * 2 + c},
             device_id_type=MESH,
         )
 
-    for c in range(2):
-        away = jnp.logical_or(e != t, tc != c)
-
-        @pl.when(away)
-        def _():
-            half_copy(c).start()
-
-        @pl.when(jnp.logical_not(away))
-        def _():
-            res_t[:, pl.ds(c * HD, HD)] = res_all[at(t, R), pl.ds(c * HD, HD)]
+    stays = jnp.logical_and(t == 0, e < 2)
+
+    @pl.when(jnp.logical_not(stays))
+    def _():
+        half_copy(0).start()
+
+    @pl.when(stays)
+    def _():
+        res_t[:, at(lax.rem(e, 2), HD)] = res_all[my_rows, 0:HD]
+
+    half_copy(1).start()
 
     load_dg.wait()
     load_du.wait()
     my_fgain = fgain_ref[:, at(e, Dc)]
+
+    def stage_a(g):
+        gy, gx = g // EX, lax.rem(g, EX)
+        dx = lax.rem(gx + EX - ex, EX)
+        return pltpu.make_async_remote_copy(
+            src_ref=dense_send.at[at(g, R), pl.ds(0, F)],
+            dst_ref=da_recv.at[dx, gy],
+            send_sem=send_a.at[g],
+            recv_sem=recv_a.at[dx * EY + gy],
+            device_id={"ep": ey * EX + gx},
+            device_id_type=MESH,
+        )
+
+    def stage_b(g):
+        gy, gx = g // EX, lax.rem(g, EX)
+        dy = lax.rem(gy + EY - ey, EY)
+        return pltpu.make_async_remote_copy(
+            src_ref=dense_send.at[at(g, R), pl.ds(F, F)],
+            dst_ref=db_recv.at[dy, gx],
+            send_sem=send_b.at[g],
+            recv_sem=recv_b.at[dy * EX + gx],
+            device_id={"ep": gy * EX + ex},
+            device_id_type=MESH,
+        )
+
+    def dense_part(tt):
+        g = lax.rem(tt + e, n_ep)
+        rows = at(g, R)
+        xg[rows, :] = (res_all[rows, :].astype(F32) * my_fgain).astype(BF16)
+        dense_send[rows, :] = dot(xg[rows, :], dgu[...]).astype(BF16)
+
+        @pl.when(lax.rem(g, EX) != ex)
+        def _():
+            stage_a(g).start()
+
+        @pl.when(g // EX != ey)
+        def _():
+            stage_b(g).start()
+
+    dense_part(t)
+    got_res[0].wait_recv()
+    dense_part(sibling)
+    late = None
+    for dz in reversed(dz_far):
+        got_res[dz].wait_recv()
+        there = lax.rem(tz + TZ - dz, TZ) * 2
+        odd = 2 * dz + 1
+        passing = side_start(
+            send_tp.at[1, odd], recv_tp.at[1, odd], res_rows(there + tc), res_rows(there + tc)
+        )
+        dense_part(there + tc)
+        if late is not None:
+            late[0].wait_recv()
+            dense_part(late[1])
+        late = (passing, there + 1 - tc)
+    late[0].wait_recv()
+    dense_part(late[1])
+
     wide_branch = branch_ref[...].astype(F32)
     pieces = Dc // LANES
     branch_rows = [
@@ -485,10 +562,7 @@
     my_branch = jnp.concatenate(branch_rows, axis=1) if pieces > 1 else branch_rows[0]
     my_branch = jnp.broadcast_to(my_branch, (8, Dc)).astype(BF16)
     ones = jnp.ones((8, Dc), BF16)
-
-    gather_tp(1, res_rows, got_res)
     block = res_all[...].astype(F32)
-    xg[...] = (block * my_fgain).astype(BF16)
     square = block * block
     high = square.astype(BF16)
     low = (square - high.astype(F32)).astype(BF16)
@@ -503,18 +577,9 @@
     stat[...] = tile
     got_stat = {k: ep_start(3, k, stat, stat_recv.at[k]) for k in ep_far}
 
-    got_dense = {}
-    for dy in dy_far:
-        rows = at(lax.rem(ey + dy, EY), RC)
-        dense_send[rows, :] = dot(xg[rows, :], dgu[...]).astype(BF16)
-        for dx in dx_far:
-            k = dy * EX + dx
-            if k:
-                got_dense[k] = ep_start(
-                    4, k, dense_send.at[at(ep_peer(k), R), :], dense_recv.at[k]
-                )
     got_disp = {}
-    for dy in dy_far:
+
+    def dispatch(dy):
         rows = at(lax.rem(ey + dy, EY), S * EX)
         disp_send[rows, :] = dot(gmat[rows, :], xg[:, at(tc, HD)]).astype(BF16)
         for dx in dx_far:
@@ -523,6 +588,50 @@
                 got_disp[k] = ep_start(
                     5, k, disp_send.at[at(ep_peer(k), S), :], xrecv.at[:, at(2 * e + tc, HD)]
                 )
+
+    for dy in dy_far[: EY // 2]:
+        dispatch(dy)
+
+    got_a, got_b = {}, {}
+    for d in dy_far:
+        gy = lax.rem(ey + d, EY)
+        term = dense_send[at(gy * EX + ex, R), 0:F].astype(F32)
+        for dx in range(1, EX):
+            pltpu.make_async_remote_copy(
+                src_ref=dense_send.at[pl.ds(0, R), pl.ds(0, F)],
+                dst_ref=da_recv.at[dx, gy],
+                send_sem=send_a.at[0],
+                recv_sem=recv_a.at[dx * EY + gy],
+                device_id={"ep": e},
+                device_id_type=MESH,
+            ).wait_recv()
+            term += da_recv[dx, gy].astype(F32)
+        if d:
+            a2_send[d] = term.astype(BF16)
+            got_a[d] = ep_start(4, d * EX, a2_send.at[d], a2_recv.at[d])
+        else:
+            g = term
+    for d in dx_far:
+        gx = lax.rem(ex + d, EX)
+        term = dense_send[at(ey * EX + gx, R), F : 2 * F].astype(F32)
+        for dy in range(1, EY):
+            pltpu.make_async_remote_copy(
+                src_ref=dense_send.at[pl.ds(0, R), pl.ds(F, F)],
+                dst_ref=db_recv.at[dy, gx],
+                send_sem=send_b.at[0],
+                recv_sem=recv_b.at[dy * EX + gx],
+                device_id={"ep": e},
+                device_id_type=MESH,
+            ).wait_recv()
+            term += db_recv[dy, gx].astype(F32)
+        if d:
+            b2_send[d] = term.astype(BF16)
+            got_b[d] = ep_start(4, d, b2_send.at[d], b2_recv.at[d])
+        else:
+            u = term
+
+    for dy in dy_far[EY // 2 :]:
+        dispatch(dy)
     xrecv[:, at(2 * e + tc, HD)] = disp_send[at(e, S), :]
 
     def forward(k):
@@ -547,12 +656,15 @@
     )
     row_scale = jnp.sum(jnp.where(row_no == my_code, scale_row, 0.0), axis=1, keepdims=True)
 
-    both = dense_send[at(e, R), :].astype(F32)
-    for k in reversed(ep_far):
-        got_dense[k].wait_recv()
-        both += dense_recv[k].astype(F32)
-    both *= my_scale
-    g, u = both[:, :F], both[:, F:]
+    for d in reversed(dy_far):
+        if d:
+            got_a[d].wait_recv()
+            g += a2_recv[d].astype(F32)
+    for d in reversed(dx_far):
+        if d:
+            got_b[d].wait_recv()
+            u += b2_recv[d].astype(F32)
+    g, u = g * my_scale, u * my_scale
     hid_all[at(e, R), :] = (g / (1.0 + jnp.exp(-g)) * u).astype(BF16)
     got_hid = {
         k: ep_start(6, k, hid_all.at[at(e, R), :], hid_all.at[at(e, R), :]) for k in ep_far
@@ -579,26 +691,40 @@
         got_yo.append(
             side_start(send_sb.at[i], recv_sb.at[i], yo_send.at[:, cols], yo_recv.at[:, cols])
         )
-    for copy, cols in zip(got_yo, strips):
+    got_fin = {}
+    wide = DH // 2
+    per_strip = max(1, wide // step)
+    for i, (copy, cols) in enumerate(zip(got_yo, strips)):
         y = dot(ehid8, edc[1, :, cols]) * row_share
         copy.wait_recv()
         y += yo_recv[:, cols].astype(F32)
         fin_send[:, :, cols] = y.reshape(n_ep, PAD, step).astype(BF16)
-    got_fin = {k: ep_start(7, k, fin_send.at[ep_peer(k)], fin_recv.at[e]) for k in ep_far}
+        if i % per_strip == per_strip - 1:
+            j = i // per_strip
+            part = pl.ds(j * per_strip * step, per_strip * step)
+            for k in ep_far:
+                got_fin[j, k] = ep_start(
+                    7 + j,
+                    k,
+                    fin_send.at[ep_peer(k), pl.ds(0, CAP), part],
+                    fin_recv.at[e, pl.ds(0, CAP), part],
+                )
     fin_recv[e] = fin_send[e]
 
     load_dd.wait()
-    for k in reversed(ep_far):
-        got_hid[k].wait_recv()
     got_no = {}
-    for dy in dy_far:
+    for dy in reversed(dy_far):
+        for dx in range(EX):
+            k = (EY - dy) % EY * EX + dx
+            if k:
+                got_hid[k].wait_recv()
         rows = at(lax.rem(ey + dy, EY), RC)
         dno_send[rows, :] = dot(hid_all[rows, :], dd[:, at(1 - tc, HD)]).astype(BF16)
         got_no[dy] = side_start(
             send_sb.at[4 + dy], recv_sb.at[4 + dy], dno_send.at[rows, :], dno_recv.at[rows, :]
         )
     got_dn = {}
-    for dy in dy_far:
+    for dy in reversed(dy_far):
         rows = at(lax.rem(ey + dy, EY), RC)
         down = dot(hid_all[rows, :], dd[:, at(tc, HD)])
         got_no[dy].wait_recv()
@@ -607,12 +733,12 @@
             k = dy * EX + dx
             if k:
                 got_dn[k] = ep_start(
-                    8, k, dn_send.at[at(ep_peer(k), R), :], dn_recv.at[:, at(e, HD)]
+                    9, k, dn_send.at[at(ep_peer(k), R), :], dn_recv.at[:, at(e, HD)]
                 )
     dn_recv[:, at(e, HD)] = dn_send[at(e, R), :]
 
-    for k in reversed(ep_far):
-        got_fin[k].wait_recv()
+    for copy in got_fin.values():
+        copy.wait_recv()
     for k in reversed(ep_far):
         got_dn[k].wait_recv()
     got_tp = {}
@@ -626,14 +752,14 @@
 
     for i in range(2):
 
-        @pl.when(jnp.logical_or(e != t, lax.rem(e, 2) != i))
+        @pl.when(jnp.logical_not(jnp.logical_and(t == 0, e == i)))
         def _():
             pltpu.make_async_remote_copy(
-                src_ref=res_all.at[at(t, R), pl.ds(0, HD)],
+                src_ref=res_all.at[pl.ds(0, R), pl.ds(0, HD)],
                 dst_ref=res_t.at[:, pl.ds(i * HD, HD)],
                 send_sem=send_tr.at[1 + i],
                 recv_sem=recv_tr.at[1 + i],
-                device_id={"ep": t, "tp": e},
+                device_id={"tp": sibling},
                 device_id_type=MESH,
             ).wait_recv()
 
@@ -650,15 +776,24 @@
     for k in ep_far:
         mix_copy(k).wait_send()
 
-    @pl.when(e != t)
+    @pl.when(t != 0)
     def _():
         mix_copy(0).wait_send()
 
-    for c in range(2):
-
-        @pl.when(jnp.logical_or(e != t, tc != c))
+    @pl.when(jnp.logical_not(stays))
+    def _():
+        half_copy(0).wait_send()
+
+    half_copy(1).wait_send()
+    for g in range(n_ep):
+
+        @pl.when(g % EX != ex)
         def _():
-            half_copy(c).wait_send()
+            stage_a(g).wait_send()
+
+        @pl.when(g // EX != ey)
+        def _():
+            stage_b(g).wait_send()
 
     gather_tp(3, out_cols, got_out)
     for b in range(n_ep):
@@ -701,6 +836,8 @@
     F = dense_gate.shape[1]
     FE = expert_gate.shape[2]
     S, S8 = CAP * n_ep, PAD * n_ep
+    EX = {16: 4, 4: 2}[n_ep]
+    EY = n_ep // EX
     vmem = pl.BlockSpec(memory_space=pltpu.VMEM)
     hbm = pl.BlockSpec(memory_space=pl.ANY)
     V = pltpu.VMEM
@@ -730,7 +867,12 @@
         V((8, LANES), F32),
         V((n_ep, 8, LANES), F32),
         V((N, 2 * F), BF16),
-        V((n_ep, R, 2 * F), BF16),
+        V((EX, EY, R, F), BF16),
+        V((EY, EX, R, F), BF16),
+        V((EY, R, F), BF16),
+        V((EY, R, F), BF16),
+        V((EX, R, F), BF16),
+        V((EX, R, F), BF16),
         V((n_ep * S, Dc // 2), BF16),
         V((S, D), BF16),
         V((N, F), BF16),
@@ -746,8 +888,8 @@
         V((n_tp // 2, R, Dc), BF16),
         V((R, D), BF16),
         pltpu.SemaphoreType.DMA((11 + 2 * n_ep,)),
-        pltpu.SemaphoreType.DMA((9, n_ep)),
-        pltpu.SemaphoreType.DMA((9, n_ep)),
+        pltpu.SemaphoreType.DMA((10, n_ep)),
+        pltpu.SemaphoreType.DMA((10, n_ep)),
         pltpu.SemaphoreType.DMA((4, n_tp)),
         pltpu.SemaphoreType.DMA((4, n_tp)),
         pltpu.SemaphoreType.DMA((n_ep,)),
@@ -758,6 +900,10 @@
         pltpu.SemaphoreType.DMA((n_ep,)),
         pltpu.SemaphoreType.DMA((8,)),
         pltpu.SemaphoreType.DMA((8,)),
+        pltpu.SemaphoreType.DMA((n_ep,)),
+        pltpu.SemaphoreType.DMA((n_ep,)),
+        pltpu.SemaphoreType.DMA((n_ep,)),
+        pltpu.SemaphoreType.DMA((n_ep,)),
     ]
     Sh = jax.ShapeDtypeStruct
     layer_out, new_norm, new_max, key_w, value, keep = pl.pallas_call(

time: 106 us -> 97.5 us (0.920)
  Pallas kernels: 100 us -> 91.9 us
    pallas_call x1, Pallas kernels: 100 us -> 91.9 us  [on_device(): pl.pallas_call(functools.partial(layer_kernel, n_ep, n_tp), out_shape=(Sh...]
where the time goes in v3:
time: 97.5 us; the launch traced here: 97.4 us
  Pallas kernels  91.9 us (94%)
  other arithmetic  2.96 us (3%)
  local copies, waits for them, and re-layouts  1.83 us (2%)
    pallas_call x1, Pallas kernels, on_device(): pl.pallas_call(functools.partial(layer_kernel, n_ep, n_tp), out_shape=(Sh...  91.9 us
    add x1, other arithmetic, on_device(): keep[:, None, None, :] * state_matrix  2.96 us

profile of v3, /device:TPU:1, one launch (start us, length us, event | category | flops | bytes accessed | tf_op | source)
XLA Modules:
  0.0 97.4 jit_solution(15797585027417562232)
XLA Ops:
  0.6 91.9 %shard_map.246 = (bf16[32,4096]{1,0:T(8,128)(2,1)}, f32[32,128]{1,0:T(8,128)}, f32[1,32]{1,0:T(1,128)}, f32[32,128]{1,0:T(8,128)}, f32[32,128]{1,0:T(8,128)}, /*index=5*/f32[32,128]{1,0:T(8,128)}) custom-call(bf16[32,4096]{1,0:T(8,128)(2,1)} %tokens_ref.1, f32[1,4096]{1,0:T(1,128)} %bitcast.16, bf16[16,4096]{1,0:T(8,128)(2,1)} %bitcast.14, ...), custom_call_target="tpu_custom_call" | custom-call | tf_op jit(solution)/shard_map/pallas_call | solution.py:909
  92.5 0.0 copy-start
  92.5 0.0 copy-start.1
  92.6 0.0 copy-start.2
  92.6 3.0 %multiply_add_fusion = f32[32,1,128,128]{3,2,1,0:T(8,128)} fusion(f32[32,1,128,128]{3,2,1,0:T(8,128)} %state_hbm.1, f32[32,128]{1,0:T(8,128)} %get-tuple-element.13, f32[32,128]{1,0:T(8,128)} %get-tuple-element.12, f32[32,128]{1,0:T(8,128)} %get-tuple-element.11), kind=kLoop, calls=%fused_computation | loop fusion | flops 1572864 | bytes 4243456 | tf_op jit(solution)/shard_map/add | solution.py:951
  95.5 0.0 copy-done
  95.5 0.7 copy.31
  96.2 0.0 copy-done.1
  96.2 0.6 copy.32
  96.8 0.0 copy-done.2
  96.9 0.5 copy.33
Async XLA Ops:
  92.5 3.0 %copy-start = (bf16[32,4096]{1,0:T(8,128)(2,1)S(1)}, bf16[32,4096]{1,0:T(8,128)(2,1)}, u32[]{:S(2)}) copy-start(bf16[32,4096]{1,0:T(8,128)(2,1)} %get-tuple-element.24) | copy-start | bytes 786436
  92.5 3.7 %copy-start.1 = (f32[32,128]{1,0:T(8,128)S(1)}, f32[32,128]{1,0:T(8,128)}, u32[]{:S(2)}) copy-start(f32[32,128]{1,0:T(8,128)} %get-tuple-element.14) | copy-start | bytes 49156
  92.6 4.3 %copy-start.2 = (f32[1,32]{1,0:T(1,128)S(1)}, f32[1,32]{1,0:T(1,128)}, u32[]{:S(2)}) copy-start(f32[1,32]{1,0:T(1,128)} %get-tuple-element.15) | copy-start | bytes 388

commit v4 on v3

--- a/solution.py
+++ b/solution.py
@@ -57,9 +57,7 @@
     out_ref,
     norm_out_ref,
     max_out_ref,
-    keyw_ref,
-    value_ref,
-    keep_ref,
+    mat_ref,
     state,
     wcat,
     wproj,
@@ -102,6 +100,7 @@
     dno_recv,
     dn_send,
     dn_recv,
+    comb,
     tp_send,
     tp_recv,
     out_all,
@@ -312,7 +311,6 @@
     keep = jnp.exp(carried - new_max)
     write = jnp.exp(g_in - new_max)
     max_out_ref[...] = jnp.sum(jnp.where(eye, new_max, 0.0), axis=0, keepdims=True)
-    keep_ref[...] = jnp.broadcast_to(keep, keep_ref.shape)
 
     for copy in load_w:
         copy.wait()
@@ -380,10 +378,12 @@
     def _():
         mix_all[:, at(t, W)] = mix_send[...]
 
+    key_t = key_w.T
+    for b in range(R):
+        state[b, 0] = keep[b : b + 1, :] * state[b, 0] + key_t[:, b : b + 1] * val[b : b + 1, :]
+    store_mat = load(state, mat_ref)
     gather_tp(0, proj_rows, got_wp)
     norm_out_ref[...] = new_norm
-    keyw_ref[...] = key_w
-    value_ref[...] = val
 
     for k in ep_far:
         got_info[k].wait_recv()
@@ -589,7 +589,7 @@
                     5, k, disp_send.at[at(ep_peer(k), S), :], xrecv.at[:, at(2 * e + tc, HD)]
                 )
 
-    for dy in dy_far[: EY // 2]:
+    for dy in dy_far:
         dispatch(dy)
 
     got_a, got_b = {}, {}
@@ -630,8 +630,6 @@
         else:
             u = term
 
-    for dy in dy_far[EY // 2 :]:
-        dispatch(dy)
     xrecv[:, at(2 * e + tc, HD)] = disp_send[at(e, S), :]
 
     def forward(k):
@@ -739,13 +737,16 @@
 
     for copy in got_fin.values():
         copy.wait_recv()
+    for z in range(TZ):
+        cols = slice(z * Dc, (z + 1) * Dc)
+        back = fin_recv[:, :, cols].astype(F32).reshape(S8, Dc).astype(BF16)
+        comb[:, cols] = dot(pick, back)
     for k in reversed(ep_far):
         got_dn[k].wait_recv()
     got_tp = {}
     for dz in dz_far + [0]:
         cols = at(lax.rem(tz + dz, TZ), Dc)
-        back = fin_recv[:, :, cols].astype(F32).reshape(S8, Dc).astype(BF16)
-        piece = dot(pick, back) + my_bshare * dn_recv[:, cols].astype(F32)
+        piece = comb[:, cols] + my_bshare * dn_recv[:, cols].astype(F32)
         tp_send[:, cols] = piece.astype(BF16)
         if dz:
             got_tp[dz] = tp_start(2, 2 * dz, tp_send.at[:, cols], tp_recv.at[dz])
@@ -801,6 +802,25 @@
             out_ref[:, pl.ds((2 * b + c) * HD, HD)] = out_all[:, pl.ds(c * DH + b * HD, HD)]
     for copy in pending:
         copy.wait_send()
+    store_mat.wait()
+
+
+def store_kernel(chunks, *refs):
+    bufs, sems = refs[8:12], refs[12]
+    rows = refs[3].shape[0] // chunks
+    moves = [(refs[i], bufs[i], refs[4 + i]) for i in range(3)]
+    for c in range(chunks):
+        part = pl.ds(c * rows, rows)
+        moves.append((refs[3].at[part], bufs[3].at[part], refs[7].at[part]))
+    inward = [pltpu.make_async_copy(m[0], m[1], sems.at[0, i]) for i, m in enumerate(moves)]
+    outward = [pltpu.make_async_copy(m[1], m[2], sems.at[1, i]) for i, m in enumerate(moves)]
+    for copy in inward:
+        copy.start()
+    for came, goes in zip(inward, outward):
+        came.wait()
+        goes.start()
+    for copy in outward:
+        copy.wait()
 
 
 def on_device(
@@ -839,7 +859,7 @@
     EX = {16: 4, 4: 2}[n_ep]
     EY = n_ep // EX
     vmem = pl.BlockSpec(memory_space=pltpu.VMEM)
-    hbm = pl.BlockSpec(memory_space=pl.ANY)
+    hbm = pl.BlockSpec(memory_space=pltpu.HBM)
     V = pltpu.VMEM
     scratch = [
         V(state_matrix.shape, F32),
@@ -884,10 +904,11 @@
         V((N, Dc // 2), BF16),
         V((N, Dc // 2), BF16),
         V((R, DH), BF16),
+        V((R, DH), F32),
         V((R, DH), BF16),
         V((n_tp // 2, R, Dc), BF16),
         V((R, D), BF16),
-        pltpu.SemaphoreType.DMA((11 + 2 * n_ep,)),
+        pltpu.SemaphoreType.DMA((12 + 2 * n_ep,)),
         pltpu.SemaphoreType.DMA((10, n_ep)),
         pltpu.SemaphoreType.DMA((10, n_ep)),
         pltpu.SemaphoreType.DMA((4, n_tp)),
@@ -906,18 +927,16 @@
         pltpu.SemaphoreType.DMA((n_ep,)),
     ]
     Sh = jax.ShapeDtypeStruct
-    layer_out, new_norm, new_max, key_w, value, keep = pl.pallas_call(
+    results = pl.pallas_call(
         functools.partial(layer_kernel, n_ep, n_tp),
         out_shape=(
             Sh((R, D), BF16),
             Sh((R, hd), F32),
             Sh((1, R), F32),
-            Sh((R, hd), F32),
-            Sh((R, hd), F32),
-            Sh((R, hd), F32),
+            Sh(state_matrix.shape, F32),
         ),
         in_specs=[vmem] * 11 + [hbm] * 12,
-        out_specs=(vmem,) * 6,
+        out_specs=(vmem,) * 3 + (hbm,),
         scratch_shapes=scratch,
         compiler_params=pltpu.CompilerParams(
             collective_id=0, has_side_effects=True, vmem_limit_bytes=66_000_000
@@ -947,9 +966,14 @@
         dense_up,
         dense_down,
     )
-    new_matrix = (
-        keep[:, None, None, :] * state_matrix + key_w[:, None, :, None] * value[:, None, None, :]
-    )
+    layer_out, new_norm, new_max, new_matrix = pl.pallas_call(
+        functools.partial(store_kernel, 8),
+        out_shape=tuple(Sh(r.shape, r.dtype) for r in results),
+        in_specs=[hbm] * 4,
+        out_specs=(hbm,) * 4,
+        scratch_shapes=[V(r.shape, r.dtype) for r in results] + [pltpu.SemaphoreType.DMA((2, 11))],
+        compiler_params=pltpu.CompilerParams(vmem_limit_bytes=66_000_000),
+    )(*results)
     return (layer_out, new_matrix, new_norm.reshape(R, 1, hd), new_max.T)
 
 

time: 97.5 us -> 92.8 us (0.952)
  other arithmetic: 2.96 us -> 0 us
  local copies, waits for them, and re-layouts: 1.83 us -> 0 us
    add x1 -> x0, other arithmetic: 2.96 us -> none  [on_device(): keep[:, None, None, :] * state_matrix]
    pallas_call x0 -> x1, Pallas kernels: none -> 2.55 us  [on_device(): pl.pallas_call(functools.partial(store_kernel, 8), out_shape=tuple((Sh(r....]
    pallas_call x1, Pallas kernels: 91.9 us -> 89.5 us  [on_device(): pl.pallas_call(functools.partial(layer_kernel, n_ep, n_tp), out_shape=(Sh...]
    unnamed x9 -> x0, local copies, waits for them, and re-layouts: 1.83 us -> none
where the time goes in v4:
time: 92.8 us; the launch traced here: 92.7 us
  Pallas kernels  92 us (99%)
    pallas_call x1, Pallas kernels, on_device(): pl.pallas_call(functools.partial(layer_kernel, n_ep, n_tp), out_shape=(Sh...  89.5 us
    pallas_call x1, Pallas kernels, on_device(): pl.pallas_call(functools.partial(store_kernel, 8), out_shape=tuple((Sh(r....  2.55 us

profile of v4, /device:TPU:1, one launch (start us, length us, event | category | flops | bytes accessed | tf_op | source)
XLA Modules:
  0.0 92.7 jit_solution(17815312669382118977)
XLA Ops:
  0.6 89.5 %shard_map.246 = (bf16[32,4096]{1,0:T(8,128)(2,1)}, f32[32,128]{1,0:T(8,128)}, f32[1,32]{1,0:T(1,128)}, f32[32,1,128,128]{3,2,1,0:T(8,128)}) custom-call(bf16[32,4096]{1,0:T(8,128)(2,1)} %tokens_ref.1, f32[1,4096]{1,0:T(1,128)} %bitcast.16, bf16[16,4096]{1,0:T(8,128)(2,1)} %bitcast.14, bf16[16,4096]{1,0:T(8,128)(2,1)} %bitcast.15, f32[1,16]{1,0:T(1,128)} %bitcast.22, ...), custom_call_target="tpu_custom_call" | custom-call | tf_op jit(solution)/shard_map/pallas_call | solution.py:930
  90.1 2.5 %shard_map.247 = (bf16[32,4096]{1,0:T(8,128)(2,1)}, f32[32,128]{1,0:T(8,128)}, f32[1,32]{1,0:T(1,128)}, f32[32,1,128,128]{3,2,1,0:T(8,128)}) custom-call(bf16[32,4096]{1,0:T(8,128)(2,1)} %get-tuple-element.12.refs_0_, f32[32,128]{1,0:T(8,128)} %get-tuple-element.13.refs_1_, f32[1,32]{1,0:T(1,128)} %get-tuple-element.14.refs_2_, ...), custom_call_target="tpu_custom_call" | custom-call | tf_op jit(solution)/shard_map/pallas_call | solution.py:969
